TPU v7x, 32 devices: a whole 2x2x4 slice. The times are simulated.
32 devices in a mesh: sp: 8 (over z, x), tp: 4 (over y, core).
Axes of the slice: x: 2, y: 2, z: 4, core: 2. Of those that a mesh axis runs over, the one named last changes fastest.
Arguments:
- tokens: bfloat16 [2048, 2048], P('sp', 'tp'), may hold values from -6 to 6
- norm_gain: float32 [2048], replicated, may hold values from 0.1 to 1.9
- query_one: bfloat16 [2048, 512], P('sp', 'tp'), may hold values from -1 to 1
- key_one: bfloat16 [2048, 512], P('sp', 'tp'), may hold values from -1 to 1
- query_two: bfloat16 [2048, 512], P('sp', 'tp'), may hold values from -0.15625 to 0.15625
- key_two: bfloat16 [2048, 512], P('sp', 'tp'), may hold values from -0.15625 to 0.15625
- value_weight: bfloat16 [2048, 1024], P('sp', 'tp'), may hold values from -0.5 to 0.5
- pool_weight: bfloat16 [2048, 1024], P('sp', 'tp'), may hold values from -0.125 to 0.125
- lambda_head: float32 [8], replicated, may hold values from 0.3 to 0.8
- head_gain: float32 [128], replicated, may hold values from 0.1 to 1.9
- group_weight: bfloat16 [8, 128, 128], replicated, may hold values from -0.5 to 0.5
- pool_scale: float32 [1024], replicated, may hold values from 0.1 to 1.9
- out_attn: bfloat16 [1024, 2048], P('tp', 'sp'), may hold values from -0.125 to 0.125
- out_pool: bfloat16 [1024, 2048], P('tp', 'sp'), may hold values from -0.125 to 0.125
Outputs:
- mixed: bfloat16 [2048, 2048], P(('sp', 'tp'))
All inputs are finite; a program needn't handle non-finite values.
Results may differ from a plain program's by a relative error of at most 0.013.
Values may be sent and summed in bfloat16 or wider, within the bound.
A program may use at most 128 MiB of HBM per device.

v0:
```python
import functools

import jax
import jax.numpy as jnp
import numpy as np
from jax import lax
from jax.experimental import pallas as pl
from jax.experimental.pallas import tpu as pltpu
from jax.sharding import PartitionSpec as P

HEAD_DIM = 64
VALUE_DIM = 128
GROUP_DIM = 128
ROPE_BASE = 500000.0
HEAD_SCALE = 0.8
NORM_FLOOR = 1e-06
HEAD_FLOOR = 0.001
MASKED = -1e30
TAIL = 16
CHUNKS = 8
PARTS = 2
MESH = pl.DeviceIdType.MESH
BF16 = jnp.bfloat16
F32 = jnp.float32


def flip(index, bit):
    return index + bit * (1 - 2 * ((index // bit) % 2))


def kernel(
    sizes,
    tok_ref,
    gain_ref,
    q1_ref,
    k1_ref,
    q2_ref,
    k2_ref,
    v_ref,
    p_ref,
    oa_ref,
    ob_ref,
    freq_ref,
    lam_ref,
    hg_ref,
    gw_ref,
    ps_ref,
    out_ref,
    wp_ref,
    op_ref,
    cos_ref,
    sin_ref,
    yacc,
    tokbuf,
    nrm,
    w_all,
    o_all,
    kv,
    q_st,
    m_st,
    l_st,
    acc_st,
    pool,
    tail,
    prior,
    cat,
    part,
    sbuf,
    rbuf,
    tok_send,
    tok_recv,
    w_up,
    w_dn,
    w_recv,
    wx_send,
    o_up,
    o_dn,
    o_recv,
    ox_send,
    kv_send,
    kv_recv,
    pp_send,
    pp_recv,
    rs_send,
    rs_recv,
):
    G, R, TP = sizes
    s = lax.axis_index("sp")
    t = lax.axis_index("tp")
    r = s // G
    g = s % G
    head = t * G + g
    other = s + 1 - 2 * g
    chunk, feats = tok_ref.shape
    rows = G * chunk
    has_up = r + 1 < R
    has_dn = r > 0

    t_bits = []
    bit = 1
    while bit < TP:
        t_bits.append(("t", bit))
        bit *= 2
    x_dim = ("g", 1)
    members = G * TP

    def member(mask):
        gg, tt = g, t
        for kind, b in mask:
            if kind == "g":
                gg = flip(gg, b)
            else:
                tt = flip(tt, b)
        return gg, tt

    def device(mask):
        gg, tt = member(mask)
        return (r * G + gg, tt)

    barrier = pltpu.get_barrier_semaphore()
    for dim in [x_dim] + t_bits:
        pl.semaphore_signal(barrier, inc=1, device_id=device([dim]), device_id_type=MESH)

    @pl.when(has_up)
    def _():
        pl.semaphore_signal(barrier, inc=1, device_id=(s + G, t), device_id_type=MESH)

    @pl.when(has_dn)
    def _():
        pl.semaphore_signal(barrier, inc=1, device_id=(s - G, t), device_id_type=MESH)

    def pack(gg):
        a, b = gg * HEAD_DIM, (gg + 1) * HEAD_DIM
        c, d = gg * VALUE_DIM, (gg + 1) * VALUE_DIM
        wp_ref[gg, :, 0:128] = jnp.concatenate([q1_ref[:, a:b], q2_ref[:, a:b]], axis=1)
        wp_ref[gg, :, 128:256] = jnp.concatenate([k1_ref[:, a:b], k2_ref[:, a:b]], axis=1)
        wp_ref[gg, :, 256:384] = v_ref[:, c:d]
        wp_ref[gg, :, 384:512] = p_ref[:, c:d]

    for gg in range(G):
        pack(gg)

    count = 1 + len(t_bits) + jnp.where(has_up, 1, 0) + jnp.where(has_dn, 1, 0)
    pl.semaphore_wait(barrier, count)

    def rdma(src, dst, ss, rs, dev):
        return pltpu.make_async_remote_copy(
            src_ref=src, dst_ref=dst, send_sem=ss, recv_sem=rs, device_id=dev, device_id_type=MESH
        )

    def up_copy(src, buf, k, up, recv):
        return rdma(src, buf.at[k], up.at[k], recv.at[k], (s + G, t))

    def dn_copy(src, buf, k, dn, recv):
        return rdma(src, buf.at[k], dn.at[k], recv.at[k], (s - G, t))

    def send_both(src, buf, k, up, dn, recv):
        @pl.when(has_up)
        def _():
            up_copy(src, buf, k, up, recv).start()

        @pl.when(has_dn)
        def _():
            dn_copy(src, buf, k, dn, recv).start()

    def cross_copy(inp, buf, xs, recv):
        return rdma(inp.at[1 - g], buf.at[s], xs, recv.at[s], (other, t))

    def wait_slot(buf, k, up, recv):
        up_copy(buf.at[k], buf, k, up, recv).wait_recv()

    def line_step(j, buf, up, dn, recv):
        for gg in (g, 1 - g):
            @pl.when(r - 1 - j >= 0)
            def _():
                k = (r - 1 - j) * G + gg
                wait_slot(buf, k, up, recv)

                @pl.when(has_up)
                def _():
                    up_copy(buf.at[k], buf, k, up, recv).start()

            @pl.when(r + 1 + j < R)
            def _():
                k = (r + 1 + j) * G + gg
                wait_slot(buf, k, up, recv)

                @pl.when(has_dn)
                def _():
                    dn_copy(buf.at[k], buf, k, dn, recv).start()

    def drain(buf, up, dn, recv):
        @pl.when(has_up)
        def _():
            @pl.loop(0, (r + 1) * G)
            def _(k):
                up_copy(buf.at[k], buf, k, up, recv).wait_send()

        @pl.when(has_dn)
        def _():
            @pl.loop(r * G, R * G)
            def _(k):
                dn_copy(buf.at[k], buf, k, dn, recv).wait_send()

    tok_dims = t_bits[1:] + [x_dim] + t_bits[:1]
    tok_stages = []
    held = [[]]
    slot = 0
    for dim in tok_dims:
        stage = []
        for mask in held:
            gg, tt = member(mask)
            src = tok_ref if not mask else tokbuf.at[gg, tt]
            stage.append((mask, src, slot))
            slot += 1
        tok_stages.append((dim, stage))
        held = held + [mask + [dim] for mask in held]

    def tok_copy(dim, mask, src, index):
        gg, tt = member(mask)
        return rdma(src, tokbuf.at[gg, tt], tok_send.at[index], tok_recv.at[index], device([dim]))

    def tok_start(i):
        dim, stage = tok_stages[i]
        for mask, src, index in stage:
            tok_copy(dim, mask, src, index).start()

    def tok_wait(i):
        dim, stage = tok_stages[i]
        for mask, src, index in stage:
            gg, tt = member(mask + [dim])
            rdma(
                tokbuf.at[gg, tt], tokbuf.at[gg, tt], tok_send.at[index], tok_recv.at[index],
                device([dim]),
            ).wait_recv()

    send_both(wp_ref.at[g], w_all, s, w_up, w_dn, w_recv)
    cross_copy(wp_ref, w_all, wx_send, w_recv).start()
    tok_start(0)
    w_all[s] = wp_ref[g]
    tokbuf[g, t] = tok_ref[...]
    for gg in range(G):
        c, d = gg * VALUE_DIM, (gg + 1) * VALUE_DIM
        op_ref[gg, :, 0:128] = oa_ref[c:d, :].T
        op_ref[gg, :, 128:256] = ob_ref[c:d, :].T
    o_all[s] = op_ref[g]

    lane128 = lax.broadcasted_iota(jnp.int32, (chunk, 2 * HEAD_DIM), 1)
    sign = jnp.where(lane128 % HEAD_DIM < HEAD_DIM // 2, -1.0, 1.0)

    @pl.loop(0, G)
    def _(b):
        at = pl.ds(pl.multiple_of(b * chunk, chunk), chunk)
        spots = r * rows + b * chunk + lax.broadcasted_iota(jnp.int32, (chunk, 2 * HEAD_DIM), 0)
        angles = spots.astype(F32) * freq_ref[...]
        cos_ref[at, :] = jnp.cos(angles)
        sin_ref[at, :] = jnp.sin(angles) * sign

    wait_slot(w_all, other, w_up, w_recv)
    send_both(w_all.at[other], w_all, other, w_up, w_dn, w_recv)
    stage_count = len(tok_stages)
    tok_wait(0)
    tok_start(1)
    cross_copy(op_ref, o_all, ox_send, o_recv).start()
    line_step(0, w_all, w_up, w_dn, w_recv)
    for i in range(1, stage_count):
        tok_wait(i)
        if i + 1 < stage_count:
            tok_start(i + 1)
            if i < R - 1:
                line_step(i, w_all, w_up, w_dn, w_recv)
    done_steps = min(stage_count - 1, R - 1)

    def start_o():
        send_both(op_ref.at[g], o_all, s, o_up, o_dn, o_recv)
        wait_slot(o_all, other, o_up, o_recv)
        send_both(o_all.at[other], o_all, other, o_up, o_dn, o_recv)

    gain = gain_ref[...]
    width = wp_ref.shape[2]
    span = nrm.shape[2]
    tile = chunk // 2

    @pl.loop(0, G * 2)
    def _(b):
        gi = b // 2
        off = pl.multiple_of((b % 2) * tile, tile)
        dst = pl.multiple_of(b * tile, tile)
        total = jnp.zeros((tile, 1), F32)
        for i in range(TP):
            x = tokbuf[gi, i, pl.ds(off, tile), :].astype(F32)
            total = total + jnp.sum(x * x, axis=-1, keepdims=True)
        inv = lax.rsqrt(total / (TP * feats) + NORM_FLOOR)
        for i in range(TP):
            x = tokbuf[gi, i, pl.ds(off, tile), :].astype(F32)
            y = (x * inv * gain[:, i * feats : (i + 1) * feats]).astype(BF16)
            for n in range(feats // span):
                nrm[i * (feats // span) + n, pl.ds(dst, tile), :] = y[:, n * span : (n + 1) * span]

    ptile = chunk

    def project(line, first):
        @pl.loop(0, rows // ptile)
        def _(b):
            at = pl.ds(pl.multiple_of(b * ptile, ptile), ptile)
            weights = w_all[pl.ds(line * G, G)].reshape(span, width)
            y = jnp.dot(nrm[line, at, :], weights, preferred_element_type=F32)
            yacc[at, :] = y if first else yacc[at, :] + y

    def project_step(j):
        @pl.when(r - 1 - j >= 0)
        def _():
            project(r - 1 - j, False)

        @pl.when(r + 1 + j < R)
        def _():
            project(r + 1 + j, False)

    project(r, True)

    @pl.loop(0, done_steps)
    def _(j):
        project_step(j)

    if done_steps < R - 1:
        @pl.loop(done_steps, R - 1)
        def _(j):
            line_step(j, w_all, w_up, w_dn, w_recv)

            @pl.when(j == R - 2)
            def _():
                start_o()

            project_step(j)
    else:
        start_o()

    def rope(x, cosine, sine):
        lane = lax.broadcasted_iota(jnp.int32, x.shape, 1)
        near = jnp.where(
            lane % HEAD_DIM < HEAD_DIM // 2,
            pltpu.roll(x, x.shape[1] - HEAD_DIM // 2, 1),
            pltpu.roll(x, HEAD_DIM // 2, 1),
        )
        return x * cosine + near * sine

    @pl.loop(0, rows // ptile)
    def _(b):
        at = pl.ds(pl.multiple_of(b * ptile, ptile), ptile)
        y = yacc[at, :]
        cosine = cos_ref[at, :]
        sine = sin_ref[at, :]
        kv[r, at, 0:128] = rope(y[:, 128:256], cosine, sine).astype(BF16)
        kv[r, at, 128:256] = y[:, 256:384].astype(BF16)
        p = y[:, 384:512].astype(BF16)
        pool[pl.ds(pl.multiple_of(TAIL + b * ptile, TAIL), ptile), :] = p.astype(F32)
        tail[...] = p[ptile - TAIL :, :]
        q = rope(y[:, 0:128], cosine, sine).astype(BF16) * jnp.array(HEAD_DIM**-0.5, BF16)
        lane = lax.broadcasted_iota(jnp.int32, q.shape, 1)
        zero = jnp.zeros_like(q)
        q_st[0, at, :] = jnp.where(lane < HEAD_DIM, q, zero)
        q_st[1, at, :] = jnp.where(lane >= HEAD_DIM, q, zero)

    def kv_copy(k):
        return rdma(kv.at[k], kv.at[k], kv_send.at[k], kv_recv.at[k], (s + G, t))

    tail_copy = rdma(tail, prior, pp_send, pp_recv, (s + G, t))

    @pl.when(has_up)
    def _():
        kv_copy(r).start()
        tail_copy.start()

    qtile = rows // 2

    def attend(k, diagonal):
        @pl.loop(0, 4)
        def _(b):
            m_index = b // 2
            at = pl.ds(pl.multiple_of((b % 2) * qtile, qtile), qtile)
            q = q_st[m_index, at, :]
            scores = lax.dot_general(
                q, kv[k, :, 0:128], (((1,), (1,)), ((), ())), preferred_element_type=F32
            )
            if diagonal:
                qpos = (b % 2) * qtile + lax.broadcasted_iota(jnp.int32, scores.shape, 0)
                kpos = lax.broadcasted_iota(jnp.int32, scores.shape, 1)
                scores = jnp.where(kpos <= qpos, scores, MASKED)
            top = jnp.max(scores, axis=-1, keepdims=True)
            if not diagonal:
                old = m_st[m_index, at, :]
                top = jnp.maximum(old, top)
                factor = jnp.exp(old - top)
            weights = jnp.exp(scores - top)
            total = jnp.sum(weights, axis=-1, keepdims=True)
            product = jnp.dot(weights.astype(BF16), kv[k, :, 128:256], preferred_element_type=F32)
            if not diagonal:
                total = total + l_st[m_index, at, :] * factor
                product = product + acc_st[m_index, at, :] * factor
            m_st[m_index, at, :] = top
            l_st[m_index, at, :] = total
            acc_st[m_index, at, :] = product

    attend(r, True)

    @pl.loop(0, R - 1)
    def _(j):
        k = r - 1 - j

        @pl.when(j < r)
        def _():
            kv_copy(k).wait_recv()

            @pl.when(has_up)
            def _():
                kv_copy(k).start()

        @pl.when(j > 0)
        def _():
            line_step(j - 1, o_all, o_up, o_dn, o_recv)

        @pl.when(j < r)
        def _():
            attend(k, False)

    @pl.when(has_dn)
    def _():
        tail_copy.wait_recv()
        pool[0:TAIL, :] = prior[...].astype(F32)

    @pl.when(r == 0)
    def _():
        pool[0:TAIL, :] = jnp.zeros((TAIL, GROUP_DIM), F32)

    ext = pool[...]
    kind = head % 4
    window = jnp.where(kind == 0, 2, jnp.where(kind == 1, 4, jnp.where(kind == 2, 8, 16)))
    run = ext + pltpu.roll(ext, 1, 0)
    chosen = run
    for power, lag in ((1, 2), (2, 4), (3, 8)):
        run = run + pltpu.roll(run, lag, 0)
        chosen = jnp.where(kind == power, run, chosen)
    spot = r * rows + lax.broadcasted_iota(jnp.int32, (rows, GROUP_DIM), 0)
    counts = jnp.minimum(spot + 1, window).astype(F32)
    mean = chosen[TAIL:, :] / counts - ext[TAIL:, :]
    mixedg = jnp.dot(mean.astype(BF16), gw_ref[head], preferred_element_type=F32)
    cat[:, 128:256] = (mixedg * ps_ref[head]).astype(BF16)

    diff = acc_st[0] / l_st[0] - lam_ref[head] * (acc_st[1] / l_st[1])
    inv = lax.rsqrt(jnp.mean(diff * diff, axis=-1, keepdims=True) + HEAD_FLOOR)
    cat[:, 0:128] = (diff * inv * hg_ref[...] * HEAD_SCALE).astype(BF16)

    share = rows // members
    half = part.shape[2]
    o_slots = o_all.shape[0] // CHUNKS
    by_line = R * PARTS == CHUNKS
    table = [sorted(range(R), key=lambda c: abs(c - i)) for i in range(R)]

    def chunk_at(k):
        if not by_line:
            return k
        total = 0
        for i in range(R):
            total = total + jnp.where(r == i, table[i][k // PARTS], 0)
        return total * PARTS + k % PARTS

    orders = ([t_bits[0], x_dim] + t_bits[1:], t_bits + [x_dim])

    def block(mask):
        gg, tt = member(mask)
        return pl.ds(pl.multiple_of((gg * TP + tt) * share, share), share)

    def combos(dims):
        found = [[]]
        for dim in dims:
            found = found + [mask + [dim] for mask in found]
        return found

    plans = []
    for h in range(CHUNKS):
        order = orders[h % 2]
        stages = []
        base = 0
        for i, dim in enumerate(order):
            masks = combos(order[i + 1 :])
            stages.append((dim, masks, base))
            base += len(masks)
        plans.append(stages)

    def rs_copy(h, dim, mask, index):
        at = block([dim] + mask)
        return rdma(
            sbuf.at[h, at, :], rbuf.at[h, index], rs_send.at[h, index], rs_recv.at[h, index],
            device([dim]),
        )

    def rs_start(h, i):
        dim, masks, base = plans[h][i]
        for n, mask in enumerate(masks):
            at = block([dim] + mask)
            sbuf[h, at, :] = part[h, at, :].astype(BF16)
        for n, mask in enumerate(masks):
            rs_copy(h, dim, mask, base + n).start()

    def rs_finish(h, i):
        dim, masks, base = plans[h][i]
        for n, mask in enumerate(masks):
            rs_copy(h, dim, mask, base + n).wait_recv()
            at = block(mask)
            part[h, at, :] = part[h, at, :] + rbuf[h, base + n].astype(F32)

    def out_product(h):
        first = chunk_at(h) * o_slots

        @pl.loop(0, 2)
        def _(b):
            at = pl.ds(pl.multiple_of(b * (rows // 2), rows // 2), rows // 2)
            columns = o_all[pl.ds(first, o_slots)].reshape(half, -1)
            part[h, at, :] = lax.dot_general(
                cat[at, :], columns, (((1,), (1,)), ((), ())), preferred_element_type=F32
            )

    levels = len(plans[0])
    mine = block([])
    last = lambda: line_step(R - 2, o_all, o_up, o_dn, o_recv)
    if by_line:
        batches = [range(CHUNKS - PARTS), range(CHUNKS - PARTS, CHUNKS)]
    else:
        batches = [range(CHUNKS)]
    def begin(batch):
        for h in batch:
            out_product(h)
            rs_start(h, 0)

    def advance(batch, i):
        for h in batch:
            rs_finish(h, i)
            if i + 1 < levels:
                rs_start(h, i + 1)
            else:
                at = pl.ds(pl.multiple_of(chunk_at(h) * half, half), half)
                out_ref[:, at] = part[h, mine, :].astype(BF16)

    if by_line:
        early, late = batches
        begin(early)
        advance(early, 0)
        last()
        begin(late)
        for i in range(1, levels):
            advance(early, i)
            advance(late, i - 1)
        advance(late, levels - 1)
    else:
        last()
        begin(batches[0])
        for i in range(levels):
            advance(batches[0], i)

    cross_copy(wp_ref, w_all, wx_send, w_recv).wait_send()
    cross_copy(op_ref, o_all, ox_send, o_recv).wait_send()
    drain(w_all, w_up, w_dn, w_recv)
    drain(o_all, o_up, o_dn, o_recv)
    for dim, stage in tok_stages:
        for mask, src, index in stage:
            tok_copy(dim, mask, src, index).wait_send()

    @pl.when(has_up)
    def _():
        tail_copy.wait_send()

        @pl.loop(0, r + 1)
        def _(k):
            kv_copy(k).wait_send()

    for h in range(CHUNKS):
        for dim, masks, base in plans[h]:
            for n, mask in enumerate(masks):
                rs_copy(h, dim, mask, base + n).wait_send()


def body(
    sp,
    tp,
    tokens,
    norm_gain,
    query_one,
    key_one,
    query_two,
    key_two,
    value_weight,
    pool_weight,
    lambda_head,
    head_gain,
    group_weight,
    pool_scale,
    out_attn,
    out_pool,
):
    G = query_one.shape[1] // HEAD_DIM
    assert G == 2 and sp % G == 0
    R = sp // G
    chunk, feats = tokens.shape
    rows = G * chunk
    depth = query_one.shape[0]
    cols = out_attn.shape[1]
    heads = lambda_head.shape[0]
    members = G * tp
    share = rows // members

    half_dim = HEAD_DIM // 2
    inverse = ROPE_BASE ** (-((np.arange(2 * HEAD_DIM) % half_dim) * 2.0 / HEAD_DIM))
    freq = jnp.asarray(inverse.astype(np.float32).reshape(1, -1))
    width = 4 * HEAD_DIM + VALUE_DIM + GROUP_DIM
    depth_out = VALUE_DIM + GROUP_DIM
    total_cols = sp * cols
    vm = pl.BlockSpec(memory_space=pltpu.VMEM)
    dma = pltpu.SemaphoreType.DMA
    return pl.pallas_call(
        functools.partial(kernel, (G, R, tp)),
        out_shape=jax.ShapeDtypeStruct((share, total_cols), BF16),
        in_specs=[vm] * 11 + [pl.BlockSpec(memory_space=pltpu.SMEM)] + [vm] * 3,
        out_specs=vm,
        scratch_shapes=[
            pltpu.VMEM((G, depth, width), BF16),
            pltpu.VMEM((G, cols, depth_out), BF16),
            pltpu.VMEM((rows, 2 * HEAD_DIM), F32),
            pltpu.VMEM((rows, 2 * HEAD_DIM), F32),
            pltpu.VMEM((rows, width), F32),
            pltpu.VMEM((G, tp, chunk, feats), BF16),
            pltpu.VMEM((R, rows, G * depth), BF16),
            pltpu.VMEM((sp, depth, width), BF16),
            pltpu.VMEM((sp, cols, depth_out), BF16),
            pltpu.VMEM((R, rows, 256), BF16),
            pltpu.VMEM((2, rows, 128), BF16),
            pltpu.VMEM((2, rows, 1), F32),
            pltpu.VMEM((2, rows, 1), F32),
            pltpu.VMEM((2, rows, VALUE_DIM), F32),
            pltpu.VMEM((TAIL + rows, GROUP_DIM), F32),
            pltpu.VMEM((TAIL, GROUP_DIM), BF16),
            pltpu.VMEM((TAIL, GROUP_DIM), BF16),
            pltpu.VMEM((rows, depth_out), BF16),
            pltpu.VMEM((CHUNKS, rows, total_cols // CHUNKS), F32),
            pltpu.VMEM((CHUNKS, rows, total_cols // CHUNKS), BF16),
            pltpu.VMEM((CHUNKS, members - 1, share, total_cols // CHUNKS), BF16),
            dma((members - 1,)),
            dma((members - 1,)),
            dma((sp,)),
            dma((sp,)),
            dma((sp,)),
            dma,
            dma((sp,)),
            dma((sp,)),
            dma((sp,)),
            dma,
            dma((R,)),
            dma((R,)),
            dma,
            dma,
            dma((CHUNKS, members - 1)),
            dma((CHUNKS, members - 1)),
        ],
        compiler_params=pltpu.CompilerParams(
            collective_id=0, has_side_effects=True, vmem_limit_bytes=58 * 1024 * 1024
        ),
    )(
        tokens,
        norm_gain.reshape(1, -1),
        query_one,
        key_one,
        query_two,
        key_two,
        value_weight,
        pool_weight,
        out_attn,
        out_pool,
        freq,
        lambda_head,
        head_gain.reshape(1, -1),
        group_weight,
        pool_scale.reshape(heads, 1, GROUP_DIM),
    )


def solution(mesh):
    in_specs = (
        P("sp", "tp"),
        P(),
        P("sp", "tp"),
        P("sp", "tp"),
        P("sp", "tp"),
        P("sp", "tp"),
        P("sp", "tp"),
        P("sp", "tp"),
        P(),
        P(),
        P(),
        P(),
        P("tp", "sp"),
        P("tp", "sp"),
    )
    return jax.shard_map(
        functools.partial(body, mesh.shape["sp"], mesh.shape["tp"]),
        mesh=mesh,
        in_specs=in_specs,
        out_specs=P(("sp", "tp"), None),
        check_vma=False,
    )
```

profile of v0, /device:TPU:24, one launch (start us, length us, event | category | flops | bytes accessed | tf_op | source)
XLA Modules:
  0.0 94.0 jit_solution(14039387853958541348)
XLA Ops:
  0.0 92.3 %shard_map.145 = bf16[64,2048]{1,0:T(8,128)(2,1)} custom-call(bf16[256,512]{1,0:T(8,128)(2,1)} %tok_ref.1, f32[1,2048]{1,0:T(1,128)} %bitcast.3, bf16[256,128]{1,0:T(8,128)(2,1)} %q1_ref.1, bf16[256,128]{1,0:T(8,128)(2,1)} %k1_ref.1, bf16[256,128]{1,0:T(8,128)(2,1)} %q2_ref.1, bf16[256,128]{1,0:T(8,128)(2,1)} %k2_ref.1, bf16[256,256]{1,0:T(8,128)(2,1)} %v_ref.1, ...), custom_call_target="tpu_custom_call" | custom-call | tf_op jit(solution)/shard_map/pallas_call | solution.py:619
  92.4 1.7 %copy.17 = bf16[64,2048]{1,0:T(8,128)(2,1)} copy(bf16[64,2048]{1,0:T(8,128)(2,1)} %shard_map.145) | data formatting | bytes 524288
where the time goes:
time: 94.2 us; the launch traced here: 94 us
  Pallas kernels  92.3 us (98%)
  local copies, waits for them, and re-layouts  1.67 us (2%)
    pallas_call x1, Pallas kernels, body(): pl.pallas_call(functools.partial(kernel, (G, R, tp)), out_shape=jax.Shape...  92.3 us

commit v1 on v0

v1 whole, which is shorter than its diff:
```python
import functools

import jax
import jax.numpy as jnp
import numpy as np
from jax import lax
from jax.experimental import pallas as pl
from jax.experimental.pallas import tpu as pltpu
from jax.sharding import PartitionSpec as P

HEAD_DIM = 64
VALUE_DIM = 128
GROUP_DIM = 128
ROPE_BASE = 500000.0
HEAD_SCALE = 0.8
NORM_FLOOR = 1e-06
HEAD_FLOOR = 0.001
MASKED = -1e30
TAIL = 16
CHUNKS = 8
PARTS = 2
XY_HOME = (True, False)
XY_PARTNER = (True, False)
MESH = pl.DeviceIdType.MESH
BF16 = jnp.bfloat16
F32 = jnp.float32


def flip(index, bit):
    return index + bit * (1 - 2 * ((index // bit) % 2))


def kernel(
    sizes,
    tok_ref,
    gain_ref,
    q1_ref,
    k1_ref,
    q2_ref,
    k2_ref,
    v_ref,
    p_ref,
    oa_ref,
    ob_ref,
    freq_ref,
    lam_ref,
    hg_ref,
    gw_ref,
    ps_ref,
    out_ref,
    wp_ref,
    op_ref,
    cos_ref,
    sin_ref,
    yacc,
    ssq,
    tokbuf,
    nrm,
    w_all,
    o_all,
    kv,
    q_st,
    m_st,
    l_st,
    acc_st,
    pool,
    tail,
    prior,
    cst,
    cat,
    part,
    sbuf,
    rbuf,
    tok_send,
    tok_recv,
    w_send,
    wx_send,
    wd_send,
    w_recv,
    o_up,
    o_dn,
    o_recv,
    ox_send,
    kv_send,
    kvd_send,
    kv_recv,
    pp_send,
    pp_recv,
    cat_send,
    cat_recv,
    rs_send,
    rs_recv,
):
    G, Q, TP = sizes
    S = 2 * G * Q
    R = 2 * Q
    s = lax.axis_index("sp")
    t = lax.axis_index("tp")
    r = s // G
    g = s % G
    q = r // 2
    b = r % 2
    y = t // 2
    c = t % 2
    other = s + 1 - 2 * g
    plane = 2 * q + c
    head = (2 * y + b) * G + g
    first = c == b
    second = c != b
    chunk, feats = tok_ref.shape
    rows = G * chunk
    has_up = r + 1 < R
    has_dn = r > 0

    def dev(q_, b_, g_, y_, c_):
        return ((2 * q_ + b_) * G + g_, 2 * y_ + c_)

    xdev = dev(q, b, 1 - g, y, c)
    ydev = dev(q, b, g, 1 - y, c)
    cdev = dev(q, b, g, y, 1 - c)

    t_bits = []
    bit = 1
    while bit < TP:
        t_bits.append(("t", bit))
        bit *= 2
    x_dim = ("g", 1)
    members = G * TP

    def member(mask):
        gg, tt = g, t
        for kind, bb in mask:
            if kind == "g":
                gg = flip(gg, bb)
            else:
                tt = flip(tt, bb)
        return gg, tt

    def device(mask):
        gg, tt = member(mask)
        return (r * G + gg, tt)

    barrier = pltpu.get_barrier_semaphore()

    def greet(where):
        pl.semaphore_signal(barrier, inc=1, device_id=where, device_id_type=MESH)

    greet(xdev)
    greet(ydev)
    greet(cdev)

    @pl.when(first)
    def _():
        greet(dev(q, b, 1 - g, y, 1 - c))
        greet(dev(q, b, g, 1 - y, 1 - c))

        @pl.loop(0, R)
        def _(p):
            @pl.when(p != r)
            def _():
                greet((p * G + g, t))

    @pl.when(second)
    def _():
        greet(dev(q, 1 - b, g, y, 0))
        greet(dev(q, 1 - b, g, y, 1))

    @pl.when(has_up)
    def _():
        greet((s + G, t))

    @pl.when(has_dn)
    def _():
        greet((s - G, t))

    @pl.loop(0, q)
    def _(e):
        greet(dev(e, b, g, y, c))

    @pl.when(jnp.logical_and(c == 0, q > 0))
    def _():
        greet(dev(q - 1, b, g, y, 1))

    def pack(gg):
        a, z = gg * HEAD_DIM, (gg + 1) * HEAD_DIM
        e, f = gg * VALUE_DIM, (gg + 1) * VALUE_DIM
        wp_ref[gg, :, 0:128] = jnp.concatenate([q1_ref[:, a:z], q2_ref[:, a:z]], axis=1)
        wp_ref[gg, :, 128:256] = jnp.concatenate([k1_ref[:, a:z], k2_ref[:, a:z]], axis=1)
        wp_ref[gg, :, 256:384] = v_ref[:, e:f]
        wp_ref[gg, :, 384:512] = p_ref[:, e:f]

    for gg in range(G):
        pack(gg)

    one = lambda flag: jnp.where(flag, 1, 0)
    last_pair = q == Q - 1
    count = 3 + 2 * one(second) + 1 + Q - one(first) + one(has_up) + one(has_dn)
    count = count + (Q - 1 - q) + one(jnp.logical_and(c == 1, q < Q - 1))
    pl.semaphore_wait(barrier, count)

    def rdma(src, dst, ss, rs, where):
        return pltpu.make_async_remote_copy(
            src_ref=src, dst_ref=dst, send_sem=ss, recv_sem=rs, device_id=where, device_id_type=MESH
        )

    cross_to = jnp.where(first, s, S)
    cross_at = jnp.where(first, other, S)

    def w_cross():
        return rdma(wp_ref.at[1 - g], w_all.at[cross_to], wx_send, w_recv.at[cross_to], xdev)

    def w_copy(kind, e):
        src = wp_ref.at[g] if kind == 0 else w_all.at[cross_at]
        slot = s if kind == 0 else other
        return rdma(
            src, w_all.at[slot], w_send.at[kind * Q + e], w_recv.at[slot], dev(e, c, g, y, c)
        )

    def w_targets(act):
        for n in range(Q):
            e = (q + 1 + n) % Q
            if n == Q - 1:
                pl.when(second)(functools.partial(act, e))
            else:
                act(e)

    def w_start(kind):
        w_targets(lambda e: w_copy(kind, e).start())

    def w_pass(slot):
        return rdma(w_all.at[slot], w_all.at[slot], wd_send.at[slot], w_recv.at[slot], cdev)

    def tok_copy(src, xx, tt, index, where):
        return rdma(src, tokbuf.at[xx, tt], tok_send.at[index], tok_recv.at[xx * TP + tt], where)

    def tok_first(index):
        where = (
            dev(q, 1 - b, g, y, b),
            dev(q, b, g, 1 - y, b),
            dev(q, b, 1 - g, y, b),
            dev(q, b, g, y, b),
        )[index]
        return tok_copy(tok_ref, g, t, index, where)

    def tok_wait(xx, tt):
        tok_copy(tokbuf.at[xx, tt], xx, tt, 0, cdev).wait_recv()

    def z_pass(k, over_y):
        tt = 2 * y + k
        return tok_copy(tokbuf.at[g, tt], g, tt, 4 + 2 * k + over_y, ydev if over_y else xdev)

    def x_pass(k):
        xx, tt = 1 - g, 2 * y + k
        return tok_copy(tokbuf.at[xx, tt], xx, tt, 8 + k, ydev)

    def y_pass(k):
        xx, tt = g, 2 * (1 - y) + k
        return tok_copy(tokbuf.at[xx, tt], xx, tt, 8 + k, xdev)

    w_cross().start()
    tok_first(0).start()
    tok_first(1).start()

    @pl.when(second)
    def _():
        tok_first(3).start()

    tok_first(2).start()
    w_start(0)

    @pl.when(first)
    def _():
        w_all[s] = wp_ref[g]
        tokbuf[g, t] = tok_ref[...]
        rdma(wp_ref.at[g], w_all.at[s], wd_send.at[s], w_recv.at[s], cdev).start()

    for gg in range(G):
        e, f = gg * VALUE_DIM, (gg + 1) * VALUE_DIM
        op_ref[gg, :, 0:128] = oa_ref[e:f, :].T
        op_ref[gg, :, 128:256] = ob_ref[e:f, :].T
    o_all[s] = op_ref[g]

    lane128 = lax.broadcasted_iota(jnp.int32, (chunk, 2 * HEAD_DIM), 1)
    sign = jnp.where(lane128 % HEAD_DIM < HEAD_DIM // 2, -1.0, 1.0)

    @pl.loop(0, G)
    def _(n):
        at = pl.ds(pl.multiple_of(n * chunk, chunk), chunk)
        spots = plane * rows + n * chunk + lax.broadcasted_iota(jnp.int32, (chunk, 2 * HEAD_DIM), 0)
        angles = spots.astype(F32) * freq_ref[...]
        cos_ref[at, :] = jnp.cos(angles)
        sin_ref[at, :] = jnp.sin(angles) * sign

    ssq[...] = jnp.zeros_like(ssq)

    def scale(xx, tt):
        at = pl.ds(pl.multiple_of(xx * chunk, chunk), chunk)
        x = tokbuf[xx, tt].astype(F32)
        ssq[at, :] = ssq[at, :] + jnp.sum(x * x, axis=-1, keepdims=True)
        nrm[tt, at, :] = (x * gain_ref[tt]).astype(BF16)

    def up_copy(src, buf, k, up, recv):
        return rdma(src, buf.at[k], up.at[k], recv.at[k], (s + G, t))

    def dn_copy(src, buf, k, dn, recv):
        return rdma(src, buf.at[k], dn.at[k], recv.at[k], (s - G, t))

    def send_both(src, buf, k, up, dn, recv):
        @pl.when(has_up)
        def _():
            up_copy(src, buf, k, up, recv).start()

        @pl.when(has_dn)
        def _():
            dn_copy(src, buf, k, dn, recv).start()

    def cross_copy(inp, buf, xs, recv):
        return rdma(inp.at[1 - g], buf.at[s], xs, recv.at[s], xdev)

    def wait_slot(buf, k, up, recv):
        up_copy(buf.at[k], buf, k, up, recv).wait_recv()

    def line_step(j, buf, up, dn, recv):
        for gg in (g, 1 - g):
            @pl.when(r - 1 - j >= 0)
            def _():
                k = (r - 1 - j) * G + gg
                wait_slot(buf, k, up, recv)

                @pl.when(has_up)
                def _():
                    up_copy(buf.at[k], buf, k, up, recv).start()

            @pl.when(r + 1 + j < R)
            def _():
                k = (r + 1 + j) * G + gg
                wait_slot(buf, k, up, recv)

                @pl.when(has_dn)
                def _():
                    dn_copy(buf.at[k], buf, k, dn, recv).start()

    def drain(buf, up, dn, recv):
        @pl.when(has_up)
        def _():
            @pl.loop(0, (r + 1) * G)
            def _(k):
                up_copy(buf.at[k], buf, k, up, recv).wait_send()

        @pl.when(has_dn)
        def _():
            @pl.loop(r * G, R * G)
            def _(k):
                dn_copy(buf.at[k], buf, k, dn, recv).wait_send()

    def w_wait(slot):
        w_pass(slot).wait_recv()

    @pl.when(second)
    def _():
        for k in range(2):
            tok_wait(g, 2 * y + k)
            z_pass(k, 1).start()
            z_pass(k, 0).start()

    @pl.when(first)
    def _():
        for k in range(2):
            tok_wait(g, 2 * (1 - y) + k)
            if not XY_HOME[k]:
                y_pass(k).start()
        tok_wait(g, 2 * y + 1 - c)

    w_wait(cross_at)
    w_start(1)
    cross_copy(op_ref, o_all, ox_send, o_recv).start()
    send_both(op_ref.at[g], o_all, s, o_up, o_dn, o_recv)

    @pl.when(first)
    def _():
        w_pass(other).start()
        for k in range(2):
            tok_wait(1 - g, 2 * y + k)
            if XY_HOME[k]:
                x_pass(k).start()

    def w_relay(gg):
        @pl.loop(1, R)
        def _(d):
            @pl.when(r - d >= 0)
            def _():
                w_wait((r - d) * G + gg)
                w_pass((r - d) * G + gg).start()

            @pl.when(r + d < R)
            def _():
                w_wait((r + d) * G + gg)
                w_pass((r + d) * G + gg).start()

    scale(g, 2 * y)
    scale(g, 2 * y + 1)

    @pl.when(first)
    def _():
        w_relay(g)

    @pl.when(second)
    def _():
        for k in range(2):
            tok_wait(g, 2 * (1 - y) + k)
            if not XY_PARTNER[k]:
                y_pass(k).start()
        for k in range(2):
            tok_wait(1 - g, 2 * y + k)
            if XY_PARTNER[k]:
                x_pass(k).start()

    for k in range(2):
        scale(g, 2 * (1 - y) + k)
        scale(1 - g, 2 * y + k)

    @pl.when(first)
    def _():
        w_relay(1 - g)

    for k in range(2):
        tok_wait(1 - g, 2 * (1 - y) + k)
        scale(1 - g, 2 * (1 - y) + k)

    @pl.when(second)
    def _():
        @pl.loop(0, S)
        def _(k):
            w_wait(k)

    width = wp_ref.shape[2]
    ptile = chunk
    group = S // TP

    @pl.loop(0, TP)
    def _(i):
        @pl.loop(0, rows // ptile)
        def _(n):
            at = pl.ds(pl.multiple_of(n * ptile, ptile), ptile)
            weights = w_all[pl.ds(i * group, group)].reshape(feats, width)
            product = jnp.dot(nrm[i, at, :], weights, preferred_element_type=F32)

            @pl.when(i == 0)
            def _():
                yacc[at, :] = product

            @pl.when(i > 0)
            def _():
                yacc[at, :] = yacc[at, :] + product

    def rope(x, cosine, sine):
        lane = lax.broadcasted_iota(jnp.int32, x.shape, 1)
        near = jnp.where(
            lane % HEAD_DIM < HEAD_DIM // 2,
            pltpu.roll(x, x.shape[1] - HEAD_DIM // 2, 1),
            pltpu.roll(x, HEAD_DIM // 2, 1),
        )
        return x * cosine + near * sine

    @pl.loop(0, rows // ptile)
    def _(n):
        at = pl.ds(pl.multiple_of(n * ptile, ptile), ptile)
        inv = lax.rsqrt(ssq[at, :] / (TP * feats) + NORM_FLOOR)
        out = yacc[at, :] * inv
        cosine = cos_ref[at, :]
        sine = sin_ref[at, :]
        kv[plane, at, 0:128] = rope(out[:, 128:256], cosine, sine).astype(BF16)
        kv[plane, at, 128:256] = out[:, 256:384].astype(BF16)
        p = out[:, 384:512].astype(BF16)
        pool[pl.ds(pl.multiple_of(TAIL + n * ptile, TAIL), ptile), :] = p.astype(F32)
        tail[...] = p[ptile - TAIL :, :]
        qq = rope(out[:, 0:128], cosine, sine).astype(BF16) * jnp.array(HEAD_DIM**-0.5, BF16)
        lane = lax.broadcasted_iota(jnp.int32, qq.shape, 1)
        zero = jnp.zeros_like(qq)
        q_st[0, at, :] = jnp.where(lane < HEAD_DIM, qq, zero)
        q_st[1, at, :] = jnp.where(lane >= HEAD_DIM, qq, zero)

    def kv_copy(e):
        return rdma(
            kv.at[plane], kv.at[plane], kv_send.at[e], kv_recv.at[plane], dev(e, b, g, y, c)
        )

    def kv_pass(e):
        k = 2 * e + c
        return rdma(kv.at[k], kv.at[k], kvd_send.at[e], kv_recv.at[k], cdev)

    def kv_wait(k):
        rdma(kv.at[k], kv.at[k], kvd_send.at[0], kv_recv.at[k], cdev).wait_recv()

    tail_copy = rdma(tail, prior, pp_send, pp_recv, (s + 2 * G * c, t + 1 - 2 * c))
    tail_out = jnp.logical_or(c == 0, q < Q - 1)
    tail_in = jnp.logical_or(c == 1, q > 0)

    @pl.loop(q + 1, Q)
    def _(e):
        kv_copy(e).start()

    @pl.when(c == 0)
    def _():
        kv_pass(q).start()

    @pl.when(tail_out)
    def _():
        tail_copy.start()

    wait_slot(o_all, other, o_up, o_recv)
    send_both(o_all.at[other], o_all, other, o_up, o_dn, o_recv)

    qtile = rows // 2

    def attend(k, diagonal):
        @pl.loop(0, 4)
        def _(n):
            m_index = n // 2
            at = pl.ds(pl.multiple_of((n % 2) * qtile, qtile), qtile)
            qq = q_st[m_index, at, :]
            scores = lax.dot_general(
                qq, kv[k, :, 0:128], (((1,), (1,)), ((), ())), preferred_element_type=F32
            )
            if diagonal:
                qpos = (n % 2) * qtile + lax.broadcasted_iota(jnp.int32, scores.shape, 0)
                kpos = lax.broadcasted_iota(jnp.int32, scores.shape, 1)
                scores = jnp.where(kpos <= qpos, scores, MASKED)
            top = jnp.max(scores, axis=-1, keepdims=True)
            if not diagonal:
                old = m_st[m_index, at, :]
                top = jnp.maximum(old, top)
                factor = jnp.exp(old - top)
            weights = jnp.exp(scores - top)
            total = jnp.sum(weights, axis=-1, keepdims=True)
            product = jnp.dot(weights.astype(BF16), kv[k, :, 128:256], preferred_element_type=F32)
            if not diagonal:
                total = total + l_st[m_index, at, :] * factor
                product = product + acc_st[m_index, at, :] * factor
            m_st[m_index, at, :] = top
            l_st[m_index, at, :] = total
            acc_st[m_index, at, :] = product

    attend(plane, True)

    @pl.when(tail_in)
    def _():
        tail_copy.wait_recv()
        pool[0:TAIL, :] = prior[...].astype(F32)

    @pl.when(jnp.logical_not(tail_in))
    def _():
        pool[0:TAIL, :] = jnp.zeros((TAIL, GROUP_DIM), F32)

    def cat_copy(i):
        return rdma(
            cst.at[i], cat.at[i], cat_send.at[i], cat_recv.at[i], dev(q, 1 - b, g, y, 1 - c)
        )

    def hand_on(i, value):
        @pl.when(first)
        def _():
            cat[i] = value

        @pl.when(second)
        def _():
            cst[i] = value
            cat_copy(i).start()

    ext = pool[...]
    kind = head % 4
    window = jnp.where(kind == 0, 2, jnp.where(kind == 1, 4, jnp.where(kind == 2, 8, 16)))
    run = ext + pltpu.roll(ext, 1, 0)
    chosen = run
    for power, lag in ((1, 2), (2, 4), (3, 8)):
        run = run + pltpu.roll(run, lag, 0)
        chosen = jnp.where(kind == power, run, chosen)
    spot = plane * rows + lax.broadcasted_iota(jnp.int32, (rows, GROUP_DIM), 0)
    counts = jnp.minimum(spot + 1, window).astype(F32)
    mean = chosen[TAIL:, :] / counts - ext[TAIL:, :]
    mixedg = jnp.dot(mean.astype(BF16), gw_ref[head], preferred_element_type=F32)
    hand_on(1, (mixedg * ps_ref[head]).astype(BF16))

    @pl.when(c == 1)
    def _():
        kv_wait(2 * q)
        attend(2 * q, False)

    line_step(0, o_all, o_up, o_dn, o_recv)

    @pl.loop(0, q)
    def _(j):
        e = q - 1 - j
        kv_wait(2 * e + c)
        kv_pass(e).start()
        attend(2 * e + c, False)
        kv_wait(2 * e + 1 - c)
        attend(2 * e + 1 - c, False)

    @pl.loop(1, R - 2)
    def _(j):
        line_step(j, o_all, o_up, o_dn, o_recv)

    diff = acc_st[0] / l_st[0] - lam_ref[head] * (acc_st[1] / l_st[1])
    inv = lax.rsqrt(jnp.mean(diff * diff, axis=-1, keepdims=True) + HEAD_FLOOR)
    hand_on(0, (diff * inv * hg_ref[...] * HEAD_SCALE).astype(BF16))

    @pl.when(second)
    def _():
        for i in range(2):
            cat_copy(i).wait_recv()

    share = rows // members
    half = part.shape[2]
    o_slots = o_all.shape[0] // CHUNKS
    by_line = R * PARTS == CHUNKS
    table = [sorted(range(R), key=lambda c: abs(c - i)) for i in range(R)]

    def chunk_at(k):
        if not by_line:
            return k
        total = 0
        for i in range(R):
            total = total + jnp.where(r == i, table[i][k // PARTS], 0)
        return total * PARTS + k % PARTS

    orders = ([t_bits[0], x_dim] + t_bits[1:], t_bits + [x_dim])

    def block(mask):
        gg, tt = member(mask)
        return pl.ds(pl.multiple_of((gg * TP + tt) * share, share), share)

    def combos(dims):
        found = [[]]
        for dim in dims:
            found = found + [mask + [dim] for mask in found]
        return found

    plans = []
    for h in range(CHUNKS):
        order = orders[h % 2]
        stages = []
        base = 0
        for i, dim in enumerate(order):
            masks = combos(order[i + 1 :])
            stages.append((dim, masks, base))
            base += len(masks)
        plans.append(stages)

    def rs_copy(h, dim, mask, index):
        at = block([dim] + mask)
        return rdma(
            sbuf.at[h, at, :], rbuf.at[h, index], rs_send.at[h, index], rs_recv.at[h, index],
            device([dim]),
        )

    def rs_start(h, i):
        dim, masks, base = plans[h][i]
        for n, mask in enumerate(masks):
            at = block([dim] + mask)
            sbuf[h, at, :] = part[h, at, :].astype(BF16)
        for n, mask in enumerate(masks):
            rs_copy(h, dim, mask, base + n).start()

    def rs_finish(h, i):
        dim, masks, base = plans[h][i]
        for n, mask in enumerate(masks):
            rs_copy(h, dim, mask, base + n).wait_recv()
            at = block(mask)
            part[h, at, :] = part[h, at, :] + rbuf[h, base + n].astype(F32)

    def out_product(h):
        first = chunk_at(h) * o_slots

        @pl.loop(0, 2)
        def _(b):
            at = pl.ds(pl.multiple_of(b * (rows // 2), rows // 2), rows // 2)
            columns = o_all[pl.ds(first, o_slots)].reshape(half, -1)
            both = jnp.concatenate([cat[0, at, :], cat[1, at, :]], axis=1)
            part[h, at, :] = lax.dot_general(
                both, columns, (((1,), (1,)), ((), ())), preferred_element_type=F32
            )

    levels = len(plans[0])
    mine = block([])
    last = lambda: line_step(R - 2, o_all, o_up, o_dn, o_recv)
    if by_line:
        batches = [range(CHUNKS - PARTS), range(CHUNKS - PARTS, CHUNKS)]
    else:
        batches = [range(CHUNKS)]
    def begin(batch):
        for h in batch:
            out_product(h)
            rs_start(h, 0)

    def advance(batch, i):
        for h in batch:
            rs_finish(h, i)
            if i + 1 < levels:
                rs_start(h, i + 1)
            else:
                at = pl.ds(pl.multiple_of(chunk_at(h) * half, half), half)
                out_ref[:, at] = part[h, mine, :].astype(BF16)

    if by_line:
        early, late = batches
        begin(early)
        advance(early, 0)
        last()
        begin(late)
        for i in range(1, levels):
            advance(early, i)
            advance(late, i - 1)
        advance(late, levels - 1)
    else:
        last()
        begin(batches[0])
        for i in range(levels):
            advance(batches[0], i)

    w_cross().wait_send()
    for kind in range(2):
        w_targets(lambda e: w_copy(kind, e).wait_send())

    @pl.when(first)
    def _():
        @pl.loop(0, S)
        def _(k):
            w_pass(k).wait_send()

    for i in range(3):
        tok_first(i).wait_send()

    @pl.when(second)
    def _():
        tok_first(3).wait_send()
        for k in range(2):
            z_pass(k, 1).wait_send()
            z_pass(k, 0).wait_send()
            (x_pass if XY_PARTNER[k] else y_pass)(k).wait_send()
            cat_copy(k).wait_send()

    @pl.when(first)
    def _():
        for k in range(2):
            (x_pass if XY_HOME[k] else y_pass)(k).wait_send()

    cross_copy(op_ref, o_all, ox_send, o_recv).wait_send()
    drain(o_all, o_up, o_dn, o_recv)

    @pl.when(tail_out)
    def _():
        tail_copy.wait_send()

    @pl.loop(q + 1, Q)
    def _(e):
        kv_copy(e).wait_send()

    @pl.loop(0, q + 1 - c)
    def _(e):
        kv_pass(e).wait_send()

    for h in range(CHUNKS):
        for dim, masks, base in plans[h]:
            for n, mask in enumerate(masks):
                rs_copy(h, dim, mask, base + n).wait_send()


def body(
    sp,
    tp,
    tokens,
    norm_gain,
    query_one,
    key_one,
    query_two,
    key_two,
    value_weight,
    pool_weight,
    lambda_head,
    head_gain,
    group_weight,
    pool_scale,
    out_attn,
    out_pool,
):
    G = query_one.shape[1] // HEAD_DIM
    assert G == 2 and tp == 2 * G and sp % (2 * G) == 0
    R = sp // G
    Q = R // 2
    chunk, feats = tokens.shape
    rows = G * chunk
    depth = query_one.shape[0]
    cols = out_attn.shape[1]
    heads = lambda_head.shape[0]
    members = G * tp
    share = rows // members

    half_dim = HEAD_DIM // 2
    inverse = ROPE_BASE ** (-((np.arange(2 * HEAD_DIM) % half_dim) * 2.0 / HEAD_DIM))
    freq = jnp.asarray(inverse.astype(np.float32).reshape(1, -1))
    width = 4 * HEAD_DIM + VALUE_DIM + GROUP_DIM
    depth_out = VALUE_DIM + GROUP_DIM
    total_cols = sp * cols
    vm = pl.BlockSpec(memory_space=pltpu.VMEM)
    dma = pltpu.SemaphoreType.DMA
    return pl.pallas_call(
        functools.partial(kernel, (G, Q, tp)),
        out_shape=jax.ShapeDtypeStruct((share, total_cols), BF16),
        in_specs=[vm] * 11 + [pl.BlockSpec(memory_space=pltpu.SMEM)] + [vm] * 3,
        out_specs=vm,
        scratch_shapes=[
            pltpu.VMEM((G, depth, width), BF16),
            pltpu.VMEM((G, cols, depth_out), BF16),
            pltpu.VMEM((rows, 2 * HEAD_DIM), F32),
            pltpu.VMEM((rows, 2 * HEAD_DIM), F32),
            pltpu.VMEM((rows, width), F32),
            pltpu.VMEM((rows, 1), F32),
            pltpu.VMEM((G, tp, chunk, feats), BF16),
            pltpu.VMEM((tp, rows, feats), BF16),
            pltpu.VMEM((sp + 1, depth, width), BF16),
            pltpu.VMEM((sp, cols, depth_out), BF16),
            pltpu.VMEM((R, rows, 256), BF16),
            pltpu.VMEM((2, rows, 128), BF16),
            pltpu.VMEM((2, rows, 1), F32),
            pltpu.VMEM((2, rows, 1), F32),
            pltpu.VMEM((2, rows, VALUE_DIM), F32),
            pltpu.VMEM((TAIL + rows, GROUP_DIM), F32),
            pltpu.VMEM((TAIL, GROUP_DIM), BF16),
            pltpu.VMEM((TAIL, GROUP_DIM), BF16),
            pltpu.VMEM((2, rows, 128), BF16),
            pltpu.VMEM((2, rows, 128), BF16),
            pltpu.VMEM((CHUNKS, rows, total_cols // CHUNKS), F32),
            pltpu.VMEM((CHUNKS, rows, total_cols // CHUNKS), BF16),
            pltpu.VMEM((CHUNKS, members - 1, share, total_cols // CHUNKS), BF16),
            dma((10,)),
            dma((members,)),
            dma((2 * Q,)),
            dma,
            dma((sp,)),
            dma((sp + 1,)),
            dma((sp,)),
            dma((sp,)),
            dma((sp,)),
            dma,
            dma((Q,)),
            dma((Q,)),
            dma((R,)),
            dma,
            dma,
            dma((2,)),
            dma((2,)),
            dma((CHUNKS, members - 1)),
            dma((CHUNKS, members - 1)),
        ],
        compiler_params=pltpu.CompilerParams(
            collective_id=0, has_side_effects=True, vmem_limit_bytes=58 * 1024 * 1024
        ),
    )(
        tokens,
        norm_gain.reshape(tp, 1, feats),
        query_one,
        key_one,
        query_two,
        key_two,
        value_weight,
        pool_weight,
        out_attn,
        out_pool,
        freq,
        lambda_head,
        head_gain.reshape(1, -1),
        group_weight,
        pool_scale.reshape(heads, 1, GROUP_DIM),
    )


def solution(mesh):
    in_specs = (
        P("sp", "tp"),
        P(),
        P("sp", "tp"),
        P("sp", "tp"),
        P("sp", "tp"),
        P("sp", "tp"),
        P("sp", "tp"),
        P("sp", "tp"),
        P(),
        P(),
        P(),
        P(),
        P("tp", "sp"),
        P("tp", "sp"),
    )
    return jax.shard_map(
        functools.partial(body, mesh.shape["sp"], mesh.shape["tp"]),
        mesh=mesh,
        in_specs=in_specs,
        out_specs=P(("sp", "tp"), None),
        check_vma=False,
    )
```

time: 94.2 us -> 83.9 us (0.89)
  the two profiles are of different devices: /device:TPU:24 before, /device:TPU:26 now
where the time goes in v1:
time: 83.9 us; the launch traced here: 83.7 us
  Pallas kernels  82 us (98%)
  local copies, waits for them, and re-layouts  1.67 us (2%)
    pallas_call x1, Pallas kernels, body(): pl.pallas_call(functools.partial(kernel, (G, Q, tp)), out_shape=jax.Shape...  82 us

profile of v1, /device:TPU:26, one launch (start us, length us, event | category | flops | bytes accessed | tf_op | source)
XLA Modules:
  0.0 83.7 jit_solution(6550349882746575973)
XLA Ops:
  0.0 82.0 %shard_map.145 = bf16[64,2048]{1,0:T(8,128)(2,1)} custom-call(bf16[256,512]{1,0:T(8,128)(2,1)} %tok_ref.1, f32[4,1,512]{2,1,0:T(1,128)} %bitcast.3, bf16[256,128]{1,0:T(8,128)(2,1)} %q1_ref.1, bf16[256,128]{1,0:T(8,128)(2,1)} %k1_ref.1, bf16[256,128]{1,0:T(8,128)(2,1)} %q2_ref.1, bf16[256,128]{1,0:T(8,128)(2,1)} %k2_ref.1, bf16[256,256]{1,0:T(8,128)(2,1)} %v_ref.1, ...), custom_call_target="tpu_custom_call" | custom-call | tf_op jit(solution)/shard_map/pallas_call | solution.py:807
  82.1 1.7 %copy.17 = bf16[64,2048]{1,0:T(8,128)(2,1)} copy(bf16[64,2048]{1,0:T(8,128)(2,1)} %shard_map.145) | data formatting | bytes 524288

commit v2 on v1

v2 whole, which is shorter than its diff:
```python
import functools

import jax
import jax.numpy as jnp
import numpy as np
from jax import lax
from jax.experimental import pallas as pl
from jax.experimental.pallas import tpu as pltpu
from jax.sharding import PartitionSpec as P

HEAD_DIM = 64
VALUE_DIM = 128
GROUP_DIM = 128
ROPE_BASE = 500000.0
HEAD_SCALE = 0.8
NORM_FLOOR = 1e-06
HEAD_FLOOR = 0.001
MASKED = -1e30
TAIL = 16
CHUNKS = 8
XY_HOME = (True, False)
XY_PARTNER = (True, False)
MESH = pl.DeviceIdType.MESH
BF16 = jnp.bfloat16
F32 = jnp.float32


def flip(index, bit):
    return index + bit * (1 - 2 * ((index // bit) % 2))


def kernel(
    sizes,
    tok_ref,
    gain_ref,
    q1_ref,
    k1_ref,
    q2_ref,
    k2_ref,
    v_ref,
    p_ref,
    oa_ref,
    ob_ref,
    freq_ref,
    lam_ref,
    hg_ref,
    gw_ref,
    ps_ref,
    out_ref,
    wp_ref,
    op_ref,
    ox_ref,
    cos_ref,
    sin_ref,
    ssq,
    tokbuf,
    nrm,
    w_all,
    o_all,
    kv,
    q_st,
    m_st,
    l_st,
    acc_st,
    pool,
    tail,
    prior,
    cat,
    part,
    sbuf,
    rbuf,
    fin,
    land,
    outb,
    tok_send,
    tok_recv,
    w_send,
    wx_send,
    wd_send,
    w_recv,
    o_send,
    od_send,
    o_recv,
    ox_send,
    ox_recv,
    kv_send,
    kvd_send,
    kv_recv,
    pp_send,
    pp_recv,
    cat_send,
    cat_recv,
    rs_send,
    rs_recv,
    fin_send,
    fin_recv,
    out_sem,
):
    G, Q, TP = sizes
    S = 2 * G * Q
    R = 2 * Q
    s = lax.axis_index("sp")
    t = lax.axis_index("tp")
    r = s // G
    g = s % G
    q = r // 2
    b = r % 2
    y = t // 2
    c = t % 2
    other = s + 1 - 2 * g
    plane = 2 * q + c
    head = (2 * y + b) * G + g
    first = c == b
    second = c != b
    chunk, feats = tok_ref.shape
    rows = G * chunk
    cols = op_ref.shape[1]
    span = G * R * cols // TP

    def half_of(p):
        return (p * G * cols // span) % 2

    def place_of(p, gg):
        start = p * G * cols
        return pl.multiple_of((start // span // 2) * span + start % span + gg * cols, cols)


    def dev(q_, b_, g_, y_, c_):
        return ((2 * q_ + b_) * G + g_, 2 * y_ + c_)

    xdev = dev(q, b, 1 - g, y, c)
    ydev = dev(q, b, g, 1 - y, c)
    cdev = dev(q, b, g, y, 1 - c)
    zdev = dev(q, 1 - b, g, y, c)

    x_dim = ("g", 1)
    y_dim = ("t", 2)
    members = 2 * G

    def member(mask):
        gg, tt = g, t
        for kind, bb in mask:
            if kind == "g":
                gg = flip(gg, bb)
            else:
                tt = flip(tt, bb)
        return gg, tt

    def device(mask):
        gg, tt = member(mask)
        return (r * G + gg, tt)

    barrier = pltpu.get_barrier_semaphore()

    def greet(where):
        pl.semaphore_signal(barrier, inc=1, device_id=where, device_id_type=MESH)

    greet(xdev)
    greet(ydev)
    greet(cdev)
    greet(zdev)

    @pl.when(first)
    def _():
        greet(dev(q, b, 1 - g, y, 1 - c))
        greet(dev(q, b, g, 1 - y, 1 - c))

        @pl.loop(0, R)
        def _(p):
            @pl.when(p != r)
            def _():
                greet((p * G + g, t))

    @pl.when(second)
    def _():
        greet(dev(q, 1 - b, g, y, 0))
        greet(dev(q, 1 - b, g, y, 1))

    @pl.loop(0, R)
    def _(p):
        @pl.when(jnp.logical_and(p != r, half_of(p) == b))
        def _():
            greet((p * G + g, t))

    @pl.loop(0, q)
    def _(e):
        greet(dev(e, b, g, y, c))

    @pl.when(jnp.logical_and(c == 0, q > 0))
    def _():
        greet(dev(q - 1, b, g, y, 1))

    def pack(gg):
        a, z = gg * HEAD_DIM, (gg + 1) * HEAD_DIM
        e, f = gg * VALUE_DIM, (gg + 1) * VALUE_DIM
        wp_ref[gg, :, 0:128] = jnp.concatenate([q1_ref[:, a:z], q2_ref[:, a:z]], axis=1)
        wp_ref[gg, :, 128:256] = jnp.concatenate([k1_ref[:, a:z], k2_ref[:, a:z]], axis=1)
        wp_ref[gg, :, 256:384] = v_ref[:, e:f]
        wp_ref[gg, :, 384:512] = p_ref[:, e:f]

    for gg in range(G):
        pack(gg)

    one = lambda flag: jnp.where(flag, 1, 0)
    count = 4 + 2 * one(second) + 1 + Q - one(first) + Q - one(half_of(r) == b)
    count = count + (Q - 1 - q) + one(jnp.logical_and(c == 1, q < Q - 1))
    pl.semaphore_wait(barrier, count)

    def rdma(src, dst, ss, rs, where):
        return pltpu.make_async_remote_copy(
            src_ref=src, dst_ref=dst, send_sem=ss, recv_sem=rs, device_id=where, device_id_type=MESH
        )

    cross_to = jnp.where(first, s, S)
    cross_at = jnp.where(first, other, S)

    def w_cross():
        return rdma(wp_ref.at[1 - g], w_all.at[cross_to], wx_send, w_recv.at[cross_to], xdev)

    def w_copy(kind, e):
        src = wp_ref.at[g] if kind == 0 else w_all.at[cross_at]
        slot = s if kind == 0 else other
        return rdma(
            src, w_all.at[slot], w_send.at[kind * Q + e], w_recv.at[slot], dev(e, c, g, y, c)
        )

    def w_targets(act):
        for n in range(Q):
            e = (q + 1 + n) % Q
            if n == Q - 1:
                pl.when(second)(functools.partial(act, e))
            else:
                act(e)

    def w_start(kind, late=None):
        def act(e):
            far = jnp.logical_and(e != q, jnp.logical_or(2 * e + c == 0, 2 * e + c == R - 1))
            if late is None:
                w_copy(kind, e).start()
            else:
                pl.when(far == late)(lambda: w_copy(kind, e).start())

        w_targets(act)

    def w_pass(slot):
        return rdma(w_all.at[slot], w_all.at[slot], wd_send.at[slot], w_recv.at[slot], cdev)

    def tok_copy(src, xx, tt, n, index, where):
        at = pl.ds(n * (chunk // 2), chunk // 2)
        return rdma(
            src.at[at, :], tokbuf.at[xx, tt, at, :], tok_send.at[2 * index + n],
            tok_recv.at[2 * (xx * TP + tt) + n], where,
        )

    def tok_first(index, n):
        where = (
            dev(q, 1 - b, g, y, b),
            dev(q, b, g, 1 - y, b),
            dev(q, b, 1 - g, y, b),
            dev(q, b, g, y, b),
        )[index]
        return tok_copy(tok_ref, g, t, n, index, where)

    def tok_wait(xx, tt, n):
        tok_copy(tokbuf.at[xx, tt], xx, tt, n, 0, cdev).wait_recv()

    def z_pass(k, over_y, n):
        tt = 2 * y + k
        return tok_copy(tokbuf.at[g, tt], g, tt, n, 4 + 2 * k + over_y, ydev if over_y else xdev)

    def x_pass(k, n):
        xx, tt = 1 - g, 2 * y + k
        return tok_copy(tokbuf.at[xx, tt], xx, tt, n, 8 + k, ydev)

    def y_pass(k, n):
        xx, tt = g, 2 * (1 - y) + k
        return tok_copy(tokbuf.at[xx, tt], xx, tt, n, 8 + k, xdev)

    w_cross().start()
    for index in range(2):
        for n in range(2):
            tok_first(index, n).start()

    @pl.when(second)
    def _():
        for n in range(2):
            tok_first(3, n).start()

    for n in range(2):
        tok_first(2, n).start()
    w_start(0, False)

    @pl.when(first)
    def _():
        w_all[s] = wp_ref[g]
        tokbuf[g, t] = tok_ref[...]
        rdma(wp_ref.at[g], w_all.at[s], wd_send.at[s], w_recv.at[s], cdev).start()

    for gg in range(G):
        e, f = gg * VALUE_DIM, (gg + 1) * VALUE_DIM
        op_ref[gg, :, 0:128] = oa_ref[e:f, :].T
        op_ref[gg, :, 128:256] = ob_ref[e:f, :].T

    def o_at(core, p, gg):
        return o_all.at[core, pl.ds(place_of(p, gg), cols), :]

    def o_copy(kind, e):
        src, gg = (op_ref.at[g], g) if kind == 0 else (ox_ref, 1 - g)
        return rdma(
            src, o_at(c, r, gg), o_send.at[kind * Q + e], o_recv.at[c * S + r * G + gg],
            dev(e, half_of(r), g, y, c),
        )

    def o_targets(act, up=None):
        for n in range(Q):
            e = (q + 1 + n) % Q
            flag = half_of(r) != b if n == Q - 1 else None
            if up is not None:
                ahead = (e > q) == up
                flag = ahead if flag is None else jnp.logical_and(flag, ahead)
            if flag is None:
                act(e)
            else:
                pl.when(flag)(functools.partial(act, e))

    def o_start(kind, up):
        o_targets(lambda e: o_copy(kind, e).start(), up)

    def o_pass(p, gg):
        at = o_at(c, p, gg)
        index = p * G + gg
        return rdma(at, at, od_send.at[index], o_recv.at[c * S + index], cdev)

    def o_wait(core, p, gg):
        at = o_at(core, p, gg)
        rdma(at, at, od_send.at[0], o_recv.at[core * S + p * G + gg], cdev).wait_recv()

    def o_own(kind):
        gg = g if kind == 0 else 1 - g

        @pl.when(half_of(r) == b)
        def _():
            o_all[c, pl.ds(place_of(r, gg), cols), :] = op_ref[g] if kind == 0 else ox_ref[...]
            rdma(
                op_ref.at[g] if kind == 0 else ox_ref, o_at(c, r, gg), od_send.at[r * G + gg],
                o_recv.at[c * S + r * G + gg], cdev,
            ).start()

    def o_cross():
        return rdma(op_ref.at[1 - g], ox_ref, ox_send, ox_recv, xdev)

    def o_relay(gg):
        @pl.loop(0, R)
        def _(p):
            @pl.when(jnp.logical_and(p != r, half_of(p) == b))
            def _():
                o_wait(c, p, gg)
                o_pass(p, gg).start()

    lane128 = lax.broadcasted_iota(jnp.int32, (chunk, 2 * HEAD_DIM), 1)
    sign = jnp.where(lane128 % HEAD_DIM < HEAD_DIM // 2, -1.0, 1.0)

    @pl.loop(0, G)
    def _(n):
        at = pl.ds(pl.multiple_of(n * chunk, chunk), chunk)
        spots = plane * rows + n * chunk + lax.broadcasted_iota(jnp.int32, (chunk, 2 * HEAD_DIM), 0)
        angles = spots.astype(F32) * freq_ref[...]
        cos_ref[at, :] = jnp.cos(angles)
        sin_ref[at, :] = jnp.sin(angles) * sign

    ssq[...] = jnp.zeros_like(ssq)

    def scale(xx, tt):
        at = pl.ds(pl.multiple_of(xx * chunk, chunk), chunk)
        x = tokbuf[xx, tt].astype(F32)
        ssq[at, :] = ssq[at, :] + jnp.sum(x * x, axis=-1, keepdims=True)
        nrm[at, pl.ds(pl.multiple_of(tt * feats, feats), feats)] = (x * gain_ref[tt]).astype(BF16)

    def w_wait(slot):
        w_pass(slot).wait_recv()

    def early_relays(n):
        @pl.when(second)
        def _():
            for k in range(2):
                tok_wait(g, 2 * y + k, n)
                z_pass(k, 1, n).start()
                z_pass(k, 0, n).start()

        @pl.when(first)
        def _():
            for k in range(2):
                tok_wait(g, 2 * (1 - y) + k, n)
                if not XY_HOME[k]:
                    y_pass(k, n).start()
            tok_wait(g, 2 * y + 1 - c, n)

    early_relays(0)
    w_start(0, True)
    early_relays(1)
    w_wait(cross_at)
    w_start(1)

    @pl.when(first)
    def _():
        w_pass(other).start()
        for n in range(2):
            for k in range(2):
                tok_wait(1 - g, 2 * y + k, n)
                if XY_HOME[k]:
                    x_pass(k, n).start()

    def w_relay(gg):
        @pl.loop(1, R)
        def _(d):
            @pl.when(r - d >= 0)
            def _():
                w_wait((r - d) * G + gg)
                w_pass((r - d) * G + gg).start()

            @pl.when(r + d < R)
            def _():
                w_wait((r + d) * G + gg)
                w_pass((r + d) * G + gg).start()

    scale(g, 2 * y)
    scale(g, 2 * y + 1)

    @pl.when(first)
    def _():
        w_relay(g)

    @pl.when(second)
    def _():
        for n in range(2):
            for k in range(2):
                tok_wait(g, 2 * (1 - y) + k, n)
                if not XY_PARTNER[k]:
                    y_pass(k, n).start()
        for n in range(2):
            for k in range(2):
                tok_wait(1 - g, 2 * y + k, n)
                if XY_PARTNER[k]:
                    x_pass(k, n).start()

    for k in range(2):
        scale(g, 2 * (1 - y) + k)
        scale(1 - g, 2 * y + k)

    @pl.when(first)
    def _():
        w_relay(1 - g)

    o_cross().start()
    o_own(0)
    for k in range(2):
        for n in range(2):
            tok_wait(1 - g, 2 * (1 - y) + k, n)
        scale(1 - g, 2 * (1 - y) + k)

    @pl.when(second)
    def _():
        @pl.loop(0, S)
        def _(k):
            w_wait(k)

    @pl.when(b == 1)
    def _():
        o_start(0, True)

    ptile = chunk

    def rope(x, cosine, sine):
        lane = lax.broadcasted_iota(jnp.int32, x.shape, 1)
        near = jnp.where(
            lane % HEAD_DIM < HEAD_DIM // 2,
            pltpu.roll(x, x.shape[1] - HEAD_DIM // 2, 1),
            pltpu.roll(x, HEAD_DIM // 2, 1),
        )
        return x * cosine + near * sine

    def kv_part(k, n):
        return kv.at[k, pl.ds(pl.multiple_of(n * ptile, ptile), ptile), :]

    def kv_copy(e, n):
        at = kv_part(plane, n)
        return rdma(at, at, kv_send.at[2 * e + n], kv_recv.at[2 * plane + n], dev(e, b, g, y, c))

    def kv_pass(e, n):
        k = 2 * e + c
        at = kv_part(k, n)
        return rdma(at, at, kvd_send.at[2 * e + n], kv_recv.at[2 * k + n], cdev)

    def kv_wait(k, n):
        at = kv_part(k, n)
        rdma(at, at, kvd_send.at[0], kv_recv.at[2 * k + n], cdev).wait_recv()

    tail_copy = rdma(tail, prior, pp_send, pp_recv, (s + 2 * G * c, t + 1 - 2 * c))
    tail_out = jnp.logical_or(c == 0, q < Q - 1)
    tail_in = jnp.logical_or(c == 1, q > 0)

    @pl.loop(0, G)
    def _(m):
        n = G - 1 - m
        at = pl.ds(pl.multiple_of(n * ptile, ptile), ptile)
        weights = w_all[0:S].reshape(TP * feats, wp_ref.shape[2])
        inv = lax.rsqrt(ssq[at, :] / (TP * feats) + NORM_FLOOR)
        out = jnp.dot(nrm[at, :], weights, preferred_element_type=F32) * inv
        cosine = cos_ref[at, :]
        sine = sin_ref[at, :]
        kv[plane, at, 0:128] = rope(out[:, 128:256], cosine, sine).astype(BF16)
        v = out[:, 256:384].astype(BF16)
        for i in range(ptile // VALUE_DIM):
            dst = pl.ds(pl.multiple_of(n * ptile + i * VALUE_DIM, VALUE_DIM), VALUE_DIM)
            kv[plane, dst, 128:256] = v[i * VALUE_DIM : (i + 1) * VALUE_DIM, :].T
        p = out[:, 384:512].astype(BF16)
        pool[pl.ds(pl.multiple_of(TAIL + n * ptile, TAIL), ptile), :] = p.astype(F32)

        @pl.when(m == 0)
        def _():
            tail[...] = p[ptile - TAIL :, :]

            @pl.when(tail_out)
            def _():
                tail_copy.start()

        @pl.loop(q + 1, Q)
        def _(e):
            kv_copy(e, n).start()

        @pl.when(c == 0)
        def _():
            kv_pass(q, n).start()

        qq = rope(out[:, 0:128], cosine, sine).astype(BF16) * jnp.array(HEAD_DIM**-0.5, BF16)
        lane = lax.broadcasted_iota(jnp.int32, qq.shape, 1)
        zero = jnp.zeros_like(qq)
        q_st[0, :, at] = jnp.where(lane < HEAD_DIM, qq, zero).T
        q_st[1, :, at] = jnp.where(lane >= HEAD_DIM, qq, zero).T

    qtile = rows // 2

    def attend(k, piece, diagonal):
        begin, size = (0, rows) if piece is None else (piece * ptile, ptile)
        keys = pl.ds(begin, size)

        @pl.loop(0, rows // qtile)
        def _(n):
            at = pl.ds(pl.multiple_of(n * qtile, qtile), qtile)
            values = jnp.concatenate(
                [
                    kv[k, pl.ds(begin + i * VALUE_DIM, VALUE_DIM), 128:256]
                    for i in range(size // VALUE_DIM)
                ],
                axis=1,
            )
            for m_index in range(2):
                scores = jnp.dot(
                    kv[k, keys, 0:128], q_st[m_index, :, at], preferred_element_type=F32
                )
                if diagonal:
                    kpos = lax.broadcasted_iota(jnp.int32, scores.shape, 0)
                    qpos = n * qtile + lax.broadcasted_iota(jnp.int32, scores.shape, 1)
                    scores = jnp.where(kpos <= qpos, scores, MASKED)
                top = jnp.max(scores, axis=0, keepdims=True)
                if not diagonal:
                    old = m_st[m_index, :, at]
                    top = jnp.maximum(old, top)
                    factor = jnp.exp(old - top)
                weights = jnp.exp(scores - top)
                total = jnp.sum(weights, axis=0, keepdims=True)
                product = jnp.dot(values, weights.astype(BF16), preferred_element_type=F32)
                if not diagonal:
                    total = total + l_st[m_index, :, at] * factor
                    product = product + acc_st[m_index, :, at] * factor
                m_st[m_index, :, at] = top
                l_st[m_index, :, at] = total
                acc_st[m_index, :, at] = product

    attend(plane, None, True)
    o_start(0, False)
    o_cross().wait_recv()
    o_start(1, False)
    o_own(1)

    @pl.when(tail_in)
    def _():
        tail_copy.wait_recv()
        pool[0:TAIL, :] = prior[...].astype(F32)

    @pl.when(jnp.logical_not(tail_in))
    def _():
        pool[0:TAIL, :] = jnp.zeros((TAIL, GROUP_DIM), F32)

    def cat_copy(i):
        return rdma(cat.at[b, i], cat.at[b, i], cat_send.at[i], cat_recv.at[i], zdev)

    def hand_on(i, value):
        cat[b, i] = value
        cat_copy(i).start()

    ext = pool[...]
    kind = head % 4
    window = jnp.where(kind == 0, 2, jnp.where(kind == 1, 4, jnp.where(kind == 2, 8, 16)))
    run = ext + pltpu.roll(ext, 1, 0)
    chosen = run
    for power, lag in ((1, 2), (2, 4), (3, 8)):
        run = run + pltpu.roll(run, lag, 0)
        chosen = jnp.where(kind == power, run, chosen)
    spot = plane * rows + lax.broadcasted_iota(jnp.int32, (rows, GROUP_DIM), 0)
    counts = jnp.minimum(spot + 1, window).astype(F32)
    mean = chosen[TAIL:, :] / counts - ext[TAIL:, :]
    mixedg = jnp.dot(mean.astype(BF16), gw_ref[head], preferred_element_type=F32)
    hand_on(1, (mixedg * ps_ref[head]).astype(BF16))

    @pl.when(c == 1)
    def _():
        for n in range(G):
            kv_wait(2 * q, n)
        attend(2 * q, None, False)


    @pl.loop(0, q)
    def _(j):
        e = q - 1 - j
        for n in reversed(range(G)):
            kv_wait(2 * e + c, n)
            kv_pass(e, n).start()
            attend(2 * e + c, n, False)
            kv_wait(2 * e + 1 - c, n)
            attend(2 * e + 1 - c, n, False)

    diff = acc_st[0] / l_st[0] - lam_ref[head] * (acc_st[1] / l_st[1])
    inv = lax.rsqrt(jnp.mean(diff * diff, axis=0, keepdims=True) + HEAD_FLOOR)
    hand_on(0, ((diff * inv).T * hg_ref[...] * HEAD_SCALE).astype(BF16))

    share = rows // members
    half = part.shape[2]
    start_at = place_of(r, 0) // half
    near = CHUNKS // Q

    def chunk_at(h):
        return (start_at + h) % CHUNKS

    def head_product(h, bb):
        both = jnp.concatenate([cat[bb, 0], cat[bb, 1]], axis=1)
        rows_at = pl.ds(pl.multiple_of(chunk_at(h) * half, half), half)
        return lax.dot_general(
            both, o_all[bb, rows_at, :], (((1,), (1,)), ((), ())), preferred_element_type=F32
        )

    for gg in range(G):
        pl.when(half_of(r) == b)(functools.partial(o_wait, 1 - c, r, gg))

    def own_product(h):
        part[h] = head_product(h, b)

    for h in range(near):
        own_product(h)
    for i in range(2):
        cat_copy(i).wait_recv()

    @pl.when(b == 0)
    def _():
        o_start(0, True)

    o_start(1, True)
    orders = ([x_dim, y_dim], [y_dim, x_dim])

    def block(mask):
        gg, tt = member(mask)
        return pl.ds(pl.multiple_of((gg * 2 + tt // 2) * share, share), share)

    def combos(dims):
        found = [[]]
        for dim in dims:
            found = found + [mask + [dim] for mask in found]
        return found

    plans = []
    for h in range(CHUNKS):
        order = orders[h % 2]
        stages = []
        base = 0
        for i, dim in enumerate(order):
            masks = combos(order[i + 1 :])
            stages.append((dim, masks, base))
            base += len(masks)
        plans.append(stages)

    def rs_copy(h, dim, mask, index):
        at = block([dim] + mask)
        return rdma(
            sbuf.at[h, at, :], rbuf.at[h, index], rs_send.at[h, index], rs_recv.at[h, index],
            device([dim]),
        )

    def rs_start(h, i):
        dim, masks, base = plans[h][i]
        for n, mask in enumerate(masks):
            at = block([dim] + mask)
            sbuf[h, at, :] = part[h, at, :].astype(BF16)
        for n, mask in enumerate(masks):
            rs_copy(h, dim, mask, base + n).start()

    def rs_finish(h, i):
        dim, masks, base = plans[h][i]
        for n, mask in enumerate(masks):
            rs_copy(h, dim, mask, base + n).wait_recv()
            at = block(mask)
            part[h, at, :] = part[h, at, :] + rbuf[h, base + n].astype(F32)

    def out_product(h, begun):
        product = head_product(h, 1 - b)
        part[h] = (part[h] if begun else head_product(h, b)) + product

    mine = block([])
    lines = share // 2

    def fin_copy(h, core):
        where = dev(q, c, g, y, core)
        at = pl.ds(pl.multiple_of(core * lines, lines), lines)
        return rdma(
            fin.at[h, at, :], land.at[b, h], fin_send.at[h, core], fin_recv.at[b, h], where
        )

    def columns(hb, h):
        start = chunk_at(h) * half
        return pl.ds(pl.multiple_of((2 * (start // span) + hb) * span + start % span, half), half)

    def put(hb, h):
        at = columns(hb, h)
        return pltpu.make_async_copy(outb.at[:, at], out_ref.at[:, at], out_sem.at[hb, h])

    for h in range(near):
        out_product(h, True)
        rs_start(h, 0)
    o_relay(g)
    o_relay(1 - g)

    @pl.loop(0, R)
    def _(p):
        @pl.when(jnp.logical_and(p != r, half_of(p) == b))
        def _():
            for gg in range(G):
                o_wait(1 - c, p, gg)

    for h in range(near, CHUNKS):
        out_product(h, False)
        rs_start(h, 0)
    for h in range(CHUNKS):
        rs_finish(h, 0)
        rs_start(h, 1)
    for h in range(CHUNKS):
        rs_finish(h, 1)
        fin[h] = part[h, mine, :].astype(BF16)

        @pl.when(first)
        def _():
            fin_copy(h, 1 - c).start()
            outb[:, columns(b, h)] = fin[h, pl.ds(pl.multiple_of(c * lines, lines), lines), :]
            put(b, h).start()

        @pl.when(second)
        def _():
            fin_copy(h, 0).start()
            fin_copy(h, 1).start()


    def take(hb, h):
        rdma(
            land.at[hb, h], land.at[hb, h], fin_send.at[h, 0], fin_recv.at[hb, h], cdev
        ).wait_recv()
        outb[:, columns(hb, h)] = land[hb, h]
        put(hb, h).start()

    for h in range(CHUNKS):
        @pl.when(second)
        def _():
            take(b, h)

        take(1 - b, h)

    w_cross().wait_send()
    for kind in range(2):
        w_targets(lambda e: w_copy(kind, e).wait_send())

    @pl.when(first)
    def _():
        @pl.loop(0, S)
        def _(k):
            w_pass(k).wait_send()

    for n in range(2):
        for i in range(3):
            tok_first(i, n).wait_send()

        @pl.when(second)
        def _():
            tok_first(3, n).wait_send()
            for k in range(2):
                z_pass(k, 1, n).wait_send()
                z_pass(k, 0, n).wait_send()
                (x_pass if XY_PARTNER[k] else y_pass)(k, n).wait_send()

        @pl.when(first)
        def _():
            for k in range(2):
                (x_pass if XY_HOME[k] else y_pass)(k, n).wait_send()

    o_cross().wait_send()
    for kind in range(2):
        o_targets(lambda e: o_copy(kind, e).wait_send())
        cat_copy(kind).wait_send()

    @pl.loop(0, R)
    def _(p):
        @pl.when(half_of(p) == b)
        def _():
            for gg in range(G):
                o_pass(p, gg).wait_send()

    @pl.when(tail_out)
    def _():
        tail_copy.wait_send()

    for n in range(G):
        @pl.loop(q + 1, Q)
        def _(e):
            kv_copy(e, n).wait_send()

        @pl.loop(0, q + 1 - c)
        def _(e):
            kv_pass(e, n).wait_send()

    for h in range(CHUNKS):
        for dim, masks, base in plans[h]:
            for n, mask in enumerate(masks):
                rs_copy(h, dim, mask, base + n).wait_send()

        @pl.when(first)
        def _():
            fin_copy(h, 1 - c).wait_send()

        @pl.when(second)
        def _():
            fin_copy(h, 0).wait_send()
            fin_copy(h, 1).wait_send()
    for h in range(CHUNKS):
        for hb in range(2):
            put(hb, h).wait()


def body(
    sp,
    tp,
    tokens,
    norm_gain,
    query_one,
    key_one,
    query_two,
    key_two,
    value_weight,
    pool_weight,
    lambda_head,
    head_gain,
    group_weight,
    pool_scale,
    out_attn,
    out_pool,
):
    G = query_one.shape[1] // HEAD_DIM
    assert G == 2 and tp == 2 * G and sp % (2 * G) == 0
    R = sp // G
    Q = R // 2
    chunk, feats = tokens.shape
    rows = G * chunk
    depth = query_one.shape[0]
    cols = out_attn.shape[1]
    heads = lambda_head.shape[0]
    members = 2 * G
    share = rows // members

    half_dim = HEAD_DIM // 2
    inverse = ROPE_BASE ** (-((np.arange(2 * HEAD_DIM) % half_dim) * 2.0 / HEAD_DIM))
    freq = jnp.asarray(inverse.astype(np.float32).reshape(1, -1))
    width = 4 * HEAD_DIM + VALUE_DIM + GROUP_DIM
    depth_out = VALUE_DIM + GROUP_DIM
    total_cols = sp * cols
    vm = pl.BlockSpec(memory_space=pltpu.VMEM)
    dma = pltpu.SemaphoreType.DMA
    return pl.pallas_call(
        functools.partial(kernel, (G, Q, tp)),
        out_shape=jax.ShapeDtypeStruct((rows // (G * tp), total_cols), BF16),
        in_specs=[vm] * 11 + [pl.BlockSpec(memory_space=pltpu.SMEM)] + [vm] * 3,
        out_specs=pl.BlockSpec(memory_space=pl.ANY),
        scratch_shapes=[
            pltpu.VMEM((G, depth, width), BF16),
            pltpu.VMEM((G, cols, depth_out), BF16),
            pltpu.VMEM((cols, depth_out), BF16),
            pltpu.VMEM((rows, 2 * HEAD_DIM), F32),
            pltpu.VMEM((rows, 2 * HEAD_DIM), F32),
            pltpu.VMEM((rows, 1), F32),
            pltpu.VMEM((G, tp, chunk, feats), BF16),
            pltpu.VMEM((rows, tp * feats), BF16),
            pltpu.VMEM((sp + 1, depth, width), BF16),
            pltpu.VMEM((2, total_cols // 2, depth_out), BF16),
            pltpu.VMEM((R, rows, 256), BF16),
            pltpu.VMEM((2, 128, rows), BF16),
            pltpu.VMEM((2, 1, rows), F32),
            pltpu.VMEM((2, 1, rows), F32),
            pltpu.VMEM((2, VALUE_DIM, rows), F32),
            pltpu.VMEM((TAIL + rows, GROUP_DIM), F32),
            pltpu.VMEM((TAIL, GROUP_DIM), BF16),
            pltpu.VMEM((TAIL, GROUP_DIM), BF16),
            pltpu.VMEM((2, 2, rows, 128), BF16),
            pltpu.VMEM((CHUNKS, rows, total_cols // 2 // CHUNKS), F32),
            pltpu.VMEM((CHUNKS, rows, total_cols // 2 // CHUNKS), BF16),
            pltpu.VMEM((CHUNKS, members - 1, share, total_cols // 2 // CHUNKS), BF16),
            pltpu.VMEM((CHUNKS, share, total_cols // 2 // CHUNKS), BF16),
            pltpu.VMEM((2, CHUNKS, share // 2, total_cols // 2 // CHUNKS), BF16),
            pltpu.VMEM((rows // (G * tp), total_cols), BF16),
            dma((20,)),
            dma((2 * G * tp,)),
            dma((2 * Q,)),
            dma,
            dma((sp,)),
            dma((sp + 1,)),
            dma((2 * Q,)),
            dma((sp,)),
            dma((2 * sp,)),
            dma,
            dma,
            dma((2 * Q,)),
            dma((2 * Q,)),
            dma((2 * R,)),
            dma,
            dma,
            dma((2,)),
            dma((2,)),
            dma((CHUNKS, members - 1)),
            dma((CHUNKS, members - 1)),
            dma((CHUNKS, 2)),
            dma((2, CHUNKS)),
            dma((2, CHUNKS)),
        ],
        compiler_params=pltpu.CompilerParams(
            collective_id=0, has_side_effects=True, vmem_limit_bytes=58 * 1024 * 1024
        ),
    )(
        tokens,
        norm_gain.reshape(tp, 1, feats),
        query_one,
        key_one,
        query_two,
        key_two,
        value_weight,
        pool_weight,
        out_attn,
        out_pool,
        freq,
        lambda_head,
        head_gain.reshape(1, -1),
        group_weight,
        pool_scale.reshape(heads, 1, GROUP_DIM),
    )


def solution(mesh):
    in_specs = (
        P("sp", "tp"),
        P(),
        P("sp", "tp"),
        P("sp", "tp"),
        P("sp", "tp"),
        P("sp", "tp"),
        P("sp", "tp"),
        P("sp", "tp"),
        P(),
        P(),
        P(),
        P(),
        P("tp", "sp"),
        P("tp", "sp"),
    )
    return jax.shard_map(
        functools.partial(body, mesh.shape["sp"], mesh.shape["tp"]),
        mesh=mesh,
        in_specs=in_specs,
        out_specs=P(("sp", "tp"), None),
        check_vma=False,
    )
```

time: 83.9 us -> 72.9 us (0.87)
  the two profiles are of different devices: /device:TPU:26 before, /device:TPU:17 now
where the time goes in v2:
time: 72.9 us; the launch traced here: 72.7 us
  Pallas kernels  71.1 us (98%)
  local copies, waits for them, and re-layouts  1.67 us (2%)
    pallas_call x1, Pallas kernels, body(): pl.pallas_call(functools.partial(kernel, (G, Q, tp)), out_shape=jax.Shape...  71.1 us
    unnamed x1, local copies, waits for them, and re-layouts  1.67 us

profile of v2, /device:TPU:17, one launch (start us, length us, event | category | flops | bytes accessed | tf_op | source)
XLA Modules:
  0.0 72.7 jit_solution(7532452654306596799)
XLA Ops:
  0.0 71.1 %shard_map.145 = bf16[64,2048]{1,0:T(8,128)(2,1)} custom-call(bf16[256,512]{1,0:T(8,128)(2,1)} %tok_ref.1, f32[4,1,512]{2,1,0:T(1,128)} %bitcast.3, bf16[256,128]{1,0:T(8,128)(2,1)} %q1_ref.1, bf16[256,128]{1,0:T(8,128)(2,1)} %k1_ref.1, bf16[256,128]{1,0:T(8,128)(2,1)} %q2_ref.1, bf16[256,128]{1,0:T(8,128)(2,1)} %k2_ref.1, bf16[256,256]{1,0:T(8,128)(2,1)} %v_ref.1, ...), custom_call_target="tpu_custom_call" | custom-call | tf_op jit(solution)/shard_map/pallas_call | solution.py:892
  71.1 1.7 %copy.17 = bf16[64,2048]{1,0:T(8,128)(2,1)} copy(bf16[64,2048]{1,0:T(8,128)(2,1)} %shard_map.145) | data formatting | bytes 524288

commit v3 on v2

--- a/solution.py
+++ b/solution.py
@@ -232,15 +232,8 @@
             else:
                 act(e)
 
-    def w_start(kind, late=None):
-        def act(e):
-            far = jnp.logical_and(e != q, jnp.logical_or(2 * e + c == 0, 2 * e + c == R - 1))
-            if late is None:
-                w_copy(kind, e).start()
-            else:
-                pl.when(far == late)(lambda: w_copy(kind, e).start())
-
-        w_targets(act)
+    def w_start(kind):
+        w_targets(lambda e: w_copy(kind, e).start())
 
     def w_pass(slot):
         return rdma(w_all.at[slot], w_all.at[slot], wd_send.at[slot], w_recv.at[slot], cdev)
@@ -288,7 +281,7 @@
 
     for n in range(2):
         tok_first(2, n).start()
-    w_start(0, False)
+    w_start(0)
 
     @pl.when(first)
     def _():
@@ -396,7 +389,6 @@
             tok_wait(g, 2 * y + 1 - c, n)
 
     early_relays(0)
-    w_start(0, True)
     early_relays(1)
     w_wait(cross_at)
     w_start(1)
@@ -463,10 +455,6 @@
         @pl.loop(0, S)
         def _(k):
             w_wait(k)
-
-    @pl.when(b == 1)
-    def _():
-        o_start(0, True)
 
     ptile = chunk
 
@@ -535,47 +523,38 @@
         qq = rope(out[:, 0:128], cosine, sine).astype(BF16) * jnp.array(HEAD_DIM**-0.5, BF16)
         lane = lax.broadcasted_iota(jnp.int32, qq.shape, 1)
         zero = jnp.zeros_like(qq)
-        q_st[0, :, at] = jnp.where(lane < HEAD_DIM, qq, zero).T
-        q_st[1, :, at] = jnp.where(lane >= HEAD_DIM, qq, zero).T
-
-    qtile = rows // 2
+        at_b = pl.ds(pl.multiple_of(rows + n * ptile, ptile), ptile)
+        q_st[:, at] = jnp.where(lane < HEAD_DIM, qq, zero).T
+        q_st[:, at_b] = jnp.where(lane >= HEAD_DIM, qq, zero).T
 
     def attend(k, piece, diagonal):
         begin, size = (0, rows) if piece is None else (piece * ptile, ptile)
-        keys = pl.ds(begin, size)
-
-        @pl.loop(0, rows // qtile)
-        def _(n):
-            at = pl.ds(pl.multiple_of(n * qtile, qtile), qtile)
-            values = jnp.concatenate(
-                [
-                    kv[k, pl.ds(begin + i * VALUE_DIM, VALUE_DIM), 128:256]
-                    for i in range(size // VALUE_DIM)
-                ],
-                axis=1,
-            )
-            for m_index in range(2):
-                scores = jnp.dot(
-                    kv[k, keys, 0:128], q_st[m_index, :, at], preferred_element_type=F32
-                )
-                if diagonal:
-                    kpos = lax.broadcasted_iota(jnp.int32, scores.shape, 0)
-                    qpos = n * qtile + lax.broadcasted_iota(jnp.int32, scores.shape, 1)
-                    scores = jnp.where(kpos <= qpos, scores, MASKED)
-                top = jnp.max(scores, axis=0, keepdims=True)
-                if not diagonal:
-                    old = m_st[m_index, :, at]
-                    top = jnp.maximum(old, top)
-                    factor = jnp.exp(old - top)
-                weights = jnp.exp(scores - top)
-                total = jnp.sum(weights, axis=0, keepdims=True)
-                product = jnp.dot(values, weights.astype(BF16), preferred_element_type=F32)
-                if not diagonal:
-                    total = total + l_st[m_index, :, at] * factor
-                    product = product + acc_st[m_index, :, at] * factor
-                m_st[m_index, :, at] = top
-                l_st[m_index, :, at] = total
-                acc_st[m_index, :, at] = product
+        values = jnp.concatenate(
+            [
+                kv[k, pl.ds(begin + i * VALUE_DIM, VALUE_DIM), 128:256]
+                for i in range(size // VALUE_DIM)
+            ],
+            axis=1,
+        )
+        scores = jnp.dot(kv[k, pl.ds(begin, size), 0:128], q_st[...], preferred_element_type=F32)
+        if diagonal:
+            kpos = lax.broadcasted_iota(jnp.int32, scores.shape, 0)
+            qpos = lax.broadcasted_iota(jnp.int32, scores.shape, 1) % rows
+            scores = jnp.where(kpos <= qpos, scores, MASKED)
+        top = jnp.max(scores, axis=0, keepdims=True)
+        if not diagonal:
+            old = m_st[...]
+            top = jnp.maximum(old, top)
+            factor = jnp.exp(old - top)
+        weights = jnp.exp(scores - top)
+        total = jnp.sum(weights, axis=0, keepdims=True)
+        product = jnp.dot(values, weights.astype(BF16), preferred_element_type=F32)
+        if not diagonal:
+            total = total + l_st[...] * factor
+            product = product + acc_st[...] * factor
+        m_st[...] = top
+        l_st[...] = total
+        acc_st[...] = product
 
     attend(plane, None, True)
     o_start(0, False)
@@ -627,10 +606,12 @@
             kv_wait(2 * e + c, n)
             kv_pass(e, n).start()
             attend(2 * e + c, n, False)
+        for n in range(G):
             kv_wait(2 * e + 1 - c, n)
-            attend(2 * e + 1 - c, n, False)
-
-    diff = acc_st[0] / l_st[0] - lam_ref[head] * (acc_st[1] / l_st[1])
+        attend(2 * e + 1 - c, None, False)
+
+    means = acc_st[...] / l_st[...]
+    diff = means[:, :rows] - lam_ref[head] * means[:, rows:]
     inv = lax.rsqrt(jnp.mean(diff * diff, axis=0, keepdims=True) + HEAD_FLOOR)
     hand_on(0, ((diff * inv).T * hg_ref[...] * HEAD_SCALE).astype(BF16))
 
@@ -657,8 +638,13 @@
 
     for h in range(near):
         own_product(h)
-    for i in range(2):
-        cat_copy(i).wait_recv()
+    cat_copy(1).wait_recv()
+
+    @pl.when(b == 1)
+    def _():
+        o_start(0, True)
+
+    cat_copy(0).wait_recv()
 
     @pl.when(b == 0)
     def _():
@@ -906,10 +892,10 @@
             pltpu.VMEM((sp + 1, depth, width), BF16),
             pltpu.VMEM((2, total_cols // 2, depth_out), BF16),
             pltpu.VMEM((R, rows, 256), BF16),
-            pltpu.VMEM((2, 128, rows), BF16),
-            pltpu.VMEM((2, 1, rows), F32),
-            pltpu.VMEM((2, 1, rows), F32),
-            pltpu.VMEM((2, VALUE_DIM, rows), F32),
+            pltpu.VMEM((128, 2 * rows), BF16),
+            pltpu.VMEM((1, 2 * rows), F32),
+            pltpu.VMEM((1, 2 * rows), F32),
+            pltpu.VMEM((VALUE_DIM, 2 * rows), F32),
             pltpu.VMEM((TAIL + rows, GROUP_DIM), F32),
             pltpu.VMEM((TAIL, GROUP_DIM), BF16),
             pltpu.VMEM((TAIL, GROUP_DIM), BF16),

time: 72.9 us -> 71.9 us (0.986)
  Pallas kernels: 71.1 us -> 70.1 us
    pallas_call x1, Pallas kernels: 71.1 us -> 70.1 us  [body(): pl.pallas_call(functools.partial(kernel, (G, Q, tp)), out_shape=jax.Shape...]
where the time goes in v3:
time: 71.9 us; the launch traced here: 71.7 us
  Pallas kernels  70.1 us (97%)
  local copies, waits for them, and re-layouts  1.67 us (2%)
    pallas_call x1, Pallas kernels, body(): pl.pallas_call(functools.partial(kernel, (G, Q, tp)), out_shape=jax.Shape...  70.1 us
    unnamed x1, local copies, waits for them, and re-layouts  1.67 us

profile of v3, /device:TPU:17, one launch (start us, length us, event | category | flops | bytes accessed | tf_op | source)
XLA Modules:
  0.0 71.7 jit_solution(3255410369504655006)
XLA Ops:
  0.0 70.1 %shard_map.145 = bf16[64,2048]{1,0:T(8,128)(2,1)} custom-call(bf16[256,512]{1,0:T(8,128)(2,1)} %tok_ref.1, f32[4,1,512]{2,1,0:T(1,128)} %bitcast.3, bf16[256,128]{1,0:T(8,128)(2,1)} %q1_ref.1, bf16[256,128]{1,0:T(8,128)(2,1)} %k1_ref.1, bf16[256,128]{1,0:T(8,128)(2,1)} %q2_ref.1, bf16[256,128]{1,0:T(8,128)(2,1)} %k2_ref.1, bf16[256,256]{1,0:T(8,128)(2,1)} %v_ref.1, ...), custom_call_target="tpu_custom_call" | custom-call | tf_op jit(solution)/shard_map/pallas_call | solution.py:878
  70.1 1.7 %copy.17 = bf16[64,2048]{1,0:T(8,128)(2,1)} copy(bf16[64,2048]{1,0:T(8,128)(2,1)} %shard_map.145) | data formatting | bytes 524288

commit v4 on v3

--- a/solution.py
+++ b/solution.py
@@ -31,8 +31,23 @@
 
 def kernel(
     sizes,
+    tok_in,
+    gain_ref,
+    q1_in,
+    k1_in,
+    q2_in,
+    k2_in,
+    v_in,
+    p_in,
+    oa_in,
+    ob_in,
+    freq_ref,
+    lam_ref,
+    hg_ref,
+    gw_in,
+    ps_ref,
+    out_ref,
     tok_ref,
-    gain_ref,
     q1_ref,
     k1_ref,
     q2_ref,
@@ -41,12 +56,7 @@
     p_ref,
     oa_ref,
     ob_ref,
-    freq_ref,
-    lam_ref,
-    hg_ref,
     gw_ref,
-    ps_ref,
-    out_ref,
     wp_ref,
     op_ref,
     ox_ref,
@@ -95,6 +105,7 @@
     fin_send,
     fin_recv,
     out_sem,
+    in_sem,
 ):
     G, Q, TP = sizes
     S = 2 * G * Q
@@ -112,7 +123,7 @@
     head = (2 * y + b) * G + g
     first = c == b
     second = c != b
-    chunk, feats = tok_ref.shape
+    chunk, feats = tok_in.shape
     rows = G * chunk
     cols = op_ref.shape[1]
     span = G * R * cols // TP
@@ -152,6 +163,19 @@
 
     barrier = pltpu.get_barrier_semaphore()
 
+    loads = [
+        pltpu.make_async_copy(src, dst, in_sem.at[i])
+        for i, (src, dst) in enumerate(
+            (
+                (k1_in, k1_ref), (k2_in, k2_ref), (v_in, v_ref), (p_in, p_ref), (q1_in, q1_ref),
+                (q2_in, q2_ref), (tok_in, tok_ref), (oa_in, oa_ref), (ob_in, ob_ref),
+                (gw_in.at[head], gw_ref),
+            )
+        )
+    ]
+    for load in loads:
+        load.start()
+
     def greet(where):
         pl.semaphore_signal(barrier, inc=1, device_id=where, device_id_type=MESH)
 
@@ -193,13 +217,16 @@
     def pack(gg):
         a, z = gg * HEAD_DIM, (gg + 1) * HEAD_DIM
         e, f = gg * VALUE_DIM, (gg + 1) * VALUE_DIM
-        wp_ref[gg, :, 0:128] = jnp.concatenate([q1_ref[:, a:z], q2_ref[:, a:z]], axis=1)
-        wp_ref[gg, :, 128:256] = jnp.concatenate([k1_ref[:, a:z], k2_ref[:, a:z]], axis=1)
-        wp_ref[gg, :, 256:384] = v_ref[:, e:f]
-        wp_ref[gg, :, 384:512] = p_ref[:, e:f]
-
+        wp_ref[gg, :, 0:128] = jnp.concatenate([k1_ref[:, a:z], k2_ref[:, a:z]], axis=1)
+        wp_ref[gg, :, 128:256] = v_ref[:, e:f]
+        wp_ref[gg, :, 256:384] = p_ref[:, e:f]
+        wp_ref[gg, :, 384:512] = jnp.concatenate([q1_ref[:, a:z], q2_ref[:, a:z]], axis=1)
+
+    for load in loads[:6]:
+        load.wait()
     for gg in range(G):
         pack(gg)
+    loads[6].wait()
 
     one = lambda flag: jnp.where(flag, 1, 0)
     count = 4 + 2 * one(second) + 1 + Q - one(first) + Q - one(half_of(r) == b)
@@ -214,14 +241,24 @@
     cross_to = jnp.where(first, s, S)
     cross_at = jnp.where(first, other, S)
 
-    def w_cross():
-        return rdma(wp_ref.at[1 - g], w_all.at[cross_to], wx_send, w_recv.at[cross_to], xdev)
-
-    def w_copy(kind, e):
-        src = wp_ref.at[g] if kind == 0 else w_all.at[cross_at]
+    early = 2 * HEAD_DIM + VALUE_DIM + GROUP_DIM
+    shares = (pl.ds(0, early), pl.ds(early, 2 * HEAD_DIM))
+    slots = S + 1
+
+    def w_cross(part_):
+        cut = shares[part_]
+        return rdma(
+            wp_ref.at[1 - g, :, cut], w_all.at[cross_to, :, cut], wx_send.at[part_],
+            w_recv.at[part_ * slots + cross_to], xdev,
+        )
+
+    def w_copy(part_, kind, e):
+        cut = shares[part_]
+        src = wp_ref.at[g, :, cut] if kind == 0 else w_all.at[cross_at, :, cut]
         slot = s if kind == 0 else other
         return rdma(
-            src, w_all.at[slot], w_send.at[kind * Q + e], w_recv.at[slot], dev(e, c, g, y, c)
+            src, w_all.at[slot, :, cut], w_send.at[(2 * part_ + kind) * Q + e],
+            w_recv.at[part_ * slots + slot], dev(e, c, g, y, c),
         )
 
     def w_targets(act):
@@ -232,11 +269,15 @@
             else:
                 act(e)
 
-    def w_start(kind):
-        w_targets(lambda e: w_copy(kind, e).start())
-
-    def w_pass(slot):
-        return rdma(w_all.at[slot], w_all.at[slot], wd_send.at[slot], w_recv.at[slot], cdev)
+    def w_start(part_, kind):
+        w_targets(lambda e: w_copy(part_, kind, e).start())
+
+    def w_pass(part_, slot, src=None):
+        at = w_all.at[slot, :, shares[part_]]
+        return rdma(
+            at if src is None else src, at, wd_send.at[part_ * S + slot],
+            w_recv.at[part_ * slots + slot], cdev,
+        )
 
     def tok_copy(src, xx, tt, n, index, where):
         at = pl.ds(n * (chunk // 2), chunk // 2)
@@ -269,7 +310,7 @@
         xx, tt = g, 2 * (1 - y) + k
         return tok_copy(tokbuf.at[xx, tt], xx, tt, n, 8 + k, xdev)
 
-    w_cross().start()
+    w_cross(0).start()
     for index in range(2):
         for n in range(2):
             tok_first(index, n).start()
@@ -279,16 +320,20 @@
         for n in range(2):
             tok_first(3, n).start()
 
-    for n in range(2):
-        tok_first(2, n).start()
-    w_start(0)
+    tok_first(2, 0).start()
+    w_cross(1).start()
+    tok_first(2, 1).start()
+    w_start(0, 0)
 
     @pl.when(first)
     def _():
         w_all[s] = wp_ref[g]
         tokbuf[g, t] = tok_ref[...]
-        rdma(wp_ref.at[g], w_all.at[s], wd_send.at[s], w_recv.at[s], cdev).start()
-
+        for i in range(2):
+            w_pass(i, s, wp_ref.at[g, :, shares[i]]).start()
+
+    for load in loads[7:]:
+        load.wait()
     for gg in range(G):
         e, f = gg * VALUE_DIM, (gg + 1) * VALUE_DIM
         op_ref[gg, :, 0:128] = oa_ref[e:f, :].T
@@ -369,8 +414,9 @@
         ssq[at, :] = ssq[at, :] + jnp.sum(x * x, axis=-1, keepdims=True)
         nrm[at, pl.ds(pl.multiple_of(tt * feats, feats), feats)] = (x * gain_ref[tt]).astype(BF16)
 
-    def w_wait(slot):
-        w_pass(slot).wait_recv()
+    def w_wait(part_, slot):
+        at = w_all.at[slot, :, shares[part_]]
+        rdma(at, at, wd_send.at[0], w_recv.at[part_ * slots + slot], cdev).wait_recv()
 
     def early_relays(n):
         @pl.when(second)
@@ -384,43 +430,49 @@
         def _():
             for k in range(2):
                 tok_wait(g, 2 * (1 - y) + k, n)
-                if not XY_HOME[k]:
-                    y_pass(k, n).start()
             tok_wait(g, 2 * y + 1 - c, n)
 
     early_relays(0)
     early_relays(1)
-    w_wait(cross_at)
-    w_start(1)
+    w_wait(0, cross_at)
+    w_start(0, 1)
+    w_start(1, 0)
 
     @pl.when(first)
     def _():
-        w_pass(other).start()
+        w_pass(0, other).start()
         for n in range(2):
             for k in range(2):
                 tok_wait(1 - g, 2 * y + k, n)
                 if XY_HOME[k]:
                     x_pass(k, n).start()
-
-    def w_relay(gg):
+            if n == 0:
+                w_wait(1, cross_at)
+                w_start(1, 1)
+
+    def w_relay(part_, gg):
         @pl.loop(1, R)
         def _(d):
             @pl.when(r - d >= 0)
             def _():
-                w_wait((r - d) * G + gg)
-                w_pass((r - d) * G + gg).start()
+                w_wait(part_, (r - d) * G + gg)
+                w_pass(part_, (r - d) * G + gg).start()
 
             @pl.when(r + d < R)
             def _():
-                w_wait((r + d) * G + gg)
-                w_pass((r + d) * G + gg).start()
+                w_wait(part_, (r + d) * G + gg)
+                w_pass(part_, (r + d) * G + gg).start()
 
     scale(g, 2 * y)
     scale(g, 2 * y + 1)
 
     @pl.when(first)
     def _():
-        w_relay(g)
+        w_relay(0, g)
+        for n in range(2):
+            for k in range(2):
+                if not XY_HOME[k]:
+                    y_pass(k, n).start()
 
     @pl.when(second)
     def _():
@@ -429,6 +481,8 @@
                 tok_wait(g, 2 * (1 - y) + k, n)
                 if not XY_PARTNER[k]:
                     y_pass(k, n).start()
+        w_wait(1, cross_at)
+        w_start(1, 1)
         for n in range(2):
             for k in range(2):
                 tok_wait(1 - g, 2 * y + k, n)
@@ -441,10 +495,11 @@
 
     @pl.when(first)
     def _():
-        w_relay(1 - g)
+        w_relay(0, 1 - g)
 
     o_cross().start()
     o_own(0)
+
     for k in range(2):
         for n in range(2):
             tok_wait(1 - g, 2 * (1 - y) + k, n)
@@ -454,7 +509,7 @@
     def _():
         @pl.loop(0, S)
         def _(k):
-            w_wait(k)
+            w_wait(0, k)
 
     ptile = chunk
 
@@ -487,21 +542,24 @@
     tail_out = jnp.logical_or(c == 0, q < Q - 1)
     tail_in = jnp.logical_or(c == 1, q > 0)
 
+    o_start(0, False)
+
+    def project(at, part_):
+        weights = w_all[0:S, :, shares[part_]].reshape(TP * feats, shares[part_].size)
+        inv = lax.rsqrt(ssq[at, :] / (TP * feats) + NORM_FLOOR)
+        return jnp.dot(nrm[at, :], weights, preferred_element_type=F32) * inv
+
     @pl.loop(0, G)
     def _(m):
         n = G - 1 - m
         at = pl.ds(pl.multiple_of(n * ptile, ptile), ptile)
-        weights = w_all[0:S].reshape(TP * feats, wp_ref.shape[2])
-        inv = lax.rsqrt(ssq[at, :] / (TP * feats) + NORM_FLOOR)
-        out = jnp.dot(nrm[at, :], weights, preferred_element_type=F32) * inv
-        cosine = cos_ref[at, :]
-        sine = sin_ref[at, :]
-        kv[plane, at, 0:128] = rope(out[:, 128:256], cosine, sine).astype(BF16)
-        v = out[:, 256:384].astype(BF16)
+        out = project(at, 0)
+        kv[plane, at, 0:128] = rope(out[:, 0:128], cos_ref[at, :], sin_ref[at, :]).astype(BF16)
+        v = out[:, 128:256].astype(BF16)
         for i in range(ptile // VALUE_DIM):
             dst = pl.ds(pl.multiple_of(n * ptile + i * VALUE_DIM, VALUE_DIM), VALUE_DIM)
             kv[plane, dst, 128:256] = v[i * VALUE_DIM : (i + 1) * VALUE_DIM, :].T
-        p = out[:, 384:512].astype(BF16)
+        p = out[:, 256:384].astype(BF16)
         pool[pl.ds(pl.multiple_of(TAIL + n * ptile, TAIL), ptile), :] = p.astype(F32)
 
         @pl.when(m == 0)
@@ -520,7 +578,27 @@
         def _():
             kv_pass(q, n).start()
 
-        qq = rope(out[:, 0:128], cosine, sine).astype(BF16) * jnp.array(HEAD_DIM**-0.5, BF16)
+    @pl.when(first)
+    def _():
+        w_pass(1, other).start()
+        w_relay(1, g)
+        w_relay(1, 1 - g)
+
+    @pl.when(second)
+    def _():
+        @pl.loop(0, S)
+        def _(k):
+            w_wait(1, k)
+
+    o_cross().wait_recv()
+    o_start(1, False)
+    o_own(1)
+
+    @pl.loop(0, G)
+    def _(n):
+        at = pl.ds(pl.multiple_of(n * ptile, ptile), ptile)
+        qq = rope(project(at, 1), cos_ref[at, :], sin_ref[at, :]).astype(BF16)
+        qq = qq * jnp.array(HEAD_DIM**-0.5, BF16)
         lane = lax.broadcasted_iota(jnp.int32, qq.shape, 1)
         zero = jnp.zeros_like(qq)
         at_b = pl.ds(pl.multiple_of(rows + n * ptile, ptile), ptile)
@@ -557,10 +635,6 @@
         acc_st[...] = product
 
     attend(plane, None, True)
-    o_start(0, False)
-    o_cross().wait_recv()
-    o_start(1, False)
-    o_own(1)
 
     @pl.when(tail_in)
     def _():
@@ -573,10 +647,6 @@
 
     def cat_copy(i):
         return rdma(cat.at[b, i], cat.at[b, i], cat_send.at[i], cat_recv.at[i], zdev)
-
-    def hand_on(i, value):
-        cat[b, i] = value
-        cat_copy(i).start()
 
     ext = pool[...]
     kind = head % 4
@@ -589,8 +659,9 @@
     spot = plane * rows + lax.broadcasted_iota(jnp.int32, (rows, GROUP_DIM), 0)
     counts = jnp.minimum(spot + 1, window).astype(F32)
     mean = chosen[TAIL:, :] / counts - ext[TAIL:, :]
-    mixedg = jnp.dot(mean.astype(BF16), gw_ref[head], preferred_element_type=F32)
-    hand_on(1, (mixedg * ps_ref[head]).astype(BF16))
+    mixedg = jnp.dot(mean.astype(BF16), gw_ref[...], preferred_element_type=F32)
+    cat[b, 1] = (mixedg * ps_ref[head]).astype(BF16)
+    cat_copy(1).start()
 
     @pl.when(c == 1)
     def _():
@@ -613,8 +684,26 @@
     means = acc_st[...] / l_st[...]
     diff = means[:, :rows] - lam_ref[head] * means[:, rows:]
     inv = lax.rsqrt(jnp.mean(diff * diff, axis=0, keepdims=True) + HEAD_FLOOR)
-    hand_on(0, ((diff * inv).T * hg_ref[...] * HEAD_SCALE).astype(BF16))
-
+    cat[b, 0] = ((diff * inv).T * hg_ref[...] * HEAD_SCALE).astype(BF16)
+    cat_copy(0).start()
+
+    for n in range(G):
+        @pl.loop(q + 1, Q)
+        def _(e):
+            kv_copy(e, n).wait_send()
+
+    def o_up():
+        @pl.when(g == 0)
+        def _():
+            o_start(0, True)
+            o_start(1, True)
+
+        @pl.when(g == 1)
+        def _():
+            o_start(1, True)
+            o_start(0, True)
+
+    o_up()
     share = rows // members
     half = part.shape[2]
     start_at = place_of(r, 0) // half
@@ -639,18 +728,7 @@
     for h in range(near):
         own_product(h)
     cat_copy(1).wait_recv()
-
-    @pl.when(b == 1)
-    def _():
-        o_start(0, True)
-
     cat_copy(0).wait_recv()
-
-    @pl.when(b == 0)
-    def _():
-        o_start(0, True)
-
-    o_start(1, True)
     orders = ([x_dim, y_dim], [y_dim, x_dim])
 
     def block(mask):
@@ -696,9 +774,8 @@
             at = block(mask)
             part[h, at, :] = part[h, at, :] + rbuf[h, base + n].astype(F32)
 
-    def out_product(h, begun):
-        product = head_product(h, 1 - b)
-        part[h] = (part[h] if begun else head_product(h, b)) + product
+    def out_product(h):
+        part[h] = head_product(h, b) + head_product(h, 1 - b)
 
     mine = block([])
     lines = share // 2
@@ -719,21 +796,25 @@
         return pltpu.make_async_copy(outb.at[:, at], out_ref.at[:, at], out_sem.at[hb, h])
 
     for h in range(near):
-        out_product(h, True)
+        part[h] = part[h] + head_product(h, 1 - b)
         rs_start(h, 0)
-    o_relay(g)
-    o_relay(1 - g)
-
-    @pl.loop(0, R)
-    def _(p):
-        @pl.when(jnp.logical_and(p != r, half_of(p) == b))
-        def _():
-            for gg in range(G):
+    def far_weights(gg):
+        o_relay(gg)
+
+        @pl.loop(0, R)
+        def _(p):
+            @pl.when(jnp.logical_and(p != r, half_of(p) == b))
+            def _():
                 o_wait(1 - c, p, gg)
 
-    for h in range(near, CHUNKS):
-        out_product(h, False)
-        rs_start(h, 0)
+    in_turn = near > 0 and cols % half == 0
+    for gg in range(G):
+        far_weights(gg)
+        if in_turn or gg == G - 1:
+            for h in range(near, CHUNKS):
+                if not in_turn or (h * half // cols) % G == gg:
+                    out_product(h)
+                    rs_start(h, 0)
     for h in range(CHUNKS):
         rs_finish(h, 0)
         rs_start(h, 1)
@@ -767,15 +848,17 @@
 
         take(1 - b, h)
 
-    w_cross().wait_send()
-    for kind in range(2):
-        w_targets(lambda e: w_copy(kind, e).wait_send())
+    for i in range(2):
+        w_cross(i).wait_send()
+        for kind in range(2):
+            w_targets(lambda e: w_copy(i, kind, e).wait_send())
 
     @pl.when(first)
     def _():
         @pl.loop(0, S)
         def _(k):
-            w_pass(k).wait_send()
+            w_pass(0, k).wait_send()
+            w_pass(1, k).wait_send()
 
     for n in range(2):
         for i in range(3):
@@ -795,9 +878,10 @@
                 (x_pass if XY_HOME[k] else y_pass)(k, n).wait_send()
 
     o_cross().wait_send()
+    for i in range(2):
+        cat_copy(i).wait_send()
     for kind in range(2):
         o_targets(lambda e: o_copy(kind, e).wait_send())
-        cat_copy(kind).wait_send()
 
     @pl.loop(0, R)
     def _(p):
@@ -811,10 +895,6 @@
         tail_copy.wait_send()
 
     for n in range(G):
-        @pl.loop(q + 1, Q)
-        def _(e):
-            kv_copy(e, n).wait_send()
-
         @pl.loop(0, q + 1 - c)
         def _(e):
             kv_pass(e, n).wait_send()
@@ -874,13 +954,24 @@
     depth_out = VALUE_DIM + GROUP_DIM
     total_cols = sp * cols
     vm = pl.BlockSpec(memory_space=pltpu.VMEM)
+    far = pl.BlockSpec(memory_space=pl.ANY)
     dma = pltpu.SemaphoreType.DMA
     return pl.pallas_call(
         functools.partial(kernel, (G, Q, tp)),
         out_shape=jax.ShapeDtypeStruct((rows // (G * tp), total_cols), BF16),
-        in_specs=[vm] * 11 + [pl.BlockSpec(memory_space=pltpu.SMEM)] + [vm] * 3,
+        in_specs=[far, vm] + [far] * 8 + [vm, pl.BlockSpec(memory_space=pltpu.SMEM), vm, far, vm],
         out_specs=pl.BlockSpec(memory_space=pl.ANY),
         scratch_shapes=[
+            pltpu.VMEM((chunk, feats), BF16),
+            pltpu.VMEM((depth, G * HEAD_DIM), BF16),
+            pltpu.VMEM((depth, G * HEAD_DIM), BF16),
+            pltpu.VMEM((depth, G * HEAD_DIM), BF16),
+            pltpu.VMEM((depth, G * HEAD_DIM), BF16),
+            pltpu.VMEM((depth, G * VALUE_DIM), BF16),
+            pltpu.VMEM((depth, G * GROUP_DIM), BF16),
+            pltpu.VMEM((G * VALUE_DIM, cols), BF16),
+            pltpu.VMEM((G * GROUP_DIM, cols), BF16),
+            pltpu.VMEM((GROUP_DIM, GROUP_DIM), BF16),
             pltpu.VMEM((G, depth, width), BF16),
             pltpu.VMEM((G, cols, depth_out), BF16),
             pltpu.VMEM((cols, depth_out), BF16),
@@ -908,10 +999,10 @@
             pltpu.VMEM((rows // (G * tp), total_cols), BF16),
             dma((20,)),
             dma((2 * G * tp,)),
-            dma((2 * Q,)),
-            dma,
-            dma((sp,)),
-            dma((sp + 1,)),
+            dma((4 * Q,)),
+            dma((2,)),
+            dma((2 * sp,)),
+            dma((2 * (sp + 1),)),
             dma((2 * Q,)),
             dma((sp,)),
             dma((2 * sp,)),
@@ -929,6 +1020,7 @@
             dma((CHUNKS, 2)),
             dma((2, CHUNKS)),
             dma((2, CHUNKS)),
+            dma((10,)),
         ],
         compiler_params=pltpu.CompilerParams(
             collective_id=0, has_side_effects=True, vmem_limit_bytes=58 * 1024 * 1024

time: 71.9 us -> 69.6 us (0.968)
  Pallas kernels: 70.1 us -> 67.8 us
    pallas_call x1, Pallas kernels: 70.1 us -> 67.8 us  [body(): pl.pallas_call(functools.partial(kernel, (G, Q, tp)), out_shape=jax.Shape...]
where the time goes in v4:
time: 69.6 us; the launch traced here: 69.4 us
  Pallas kernels  67.8 us (97%)
  local copies, waits for them, and re-layouts  1.67 us (2%)
    pallas_call x1, Pallas kernels, body(): pl.pallas_call(functools.partial(kernel, (G, Q, tp)), out_shape=jax.Shape...  67.8 us
    unnamed x1, local copies, waits for them, and re-layouts  1.67 us

profile of v4, /device:TPU:17, one launch (start us, length us, event | category | flops | bytes accessed | tf_op | source)
XLA Modules:
  0.0 69.4 jit_solution(14284037114543664646)
XLA Ops:
  0.0 67.8 %shard_map.145 = bf16[64,2048]{1,0:T(8,128)(2,1)} custom-call(bf16[256,512]{1,0:T(8,128)(2,1)} %tok_in.1, f32[4,1,512]{2,1,0:T(1,128)} %bitcast.3, bf16[256,128]{1,0:T(8,128)(2,1)} %q1_in.1, bf16[256,128]{1,0:T(8,128)(2,1)} %k1_in.1, bf16[256,128]{1,0:T(8,128)(2,1)} %q2_in.1, bf16[256,128]{1,0:T(8,128)(2,1)} %k2_in.1, bf16[256,256]{1,0:T(8,128)(2,1)} %v_in.1, ...), custom_call_target="tpu_custom_call" | custom-call | tf_op jit(solution)/shard_map/pallas_call | solution.py:959
  67.8 1.7 %copy.17 = bf16[64,2048]{1,0:T(8,128)(2,1)} copy(bf16[64,2048]{1,0:T(8,128)(2,1)} %shard_map.145) | data formatting | bytes 524288

commit v5 on v4

--- a/solution.py
+++ b/solution.py
@@ -173,7 +173,7 @@
             )
         )
     ]
-    for load in loads:
+    for load in loads[:7]:
         load.start()
 
     def greet(where):
@@ -183,6 +183,8 @@
     greet(ydev)
     greet(cdev)
     greet(zdev)
+    greet(dev(q, 1 - b, 1 - g, y, b))
+    greet(dev(q, 1 - b, g, 1 - y, b))
 
     @pl.when(first)
     def _():
@@ -227,9 +229,11 @@
     for gg in range(G):
         pack(gg)
     loads[6].wait()
+    for load in loads[7:]:
+        load.start()
 
     one = lambda flag: jnp.where(flag, 1, 0)
-    count = 4 + 2 * one(second) + 1 + Q - one(first) + Q - one(half_of(r) == b)
+    count = 4 + 6 * one(second) + 1 + Q - one(first) + Q - one(half_of(r) == b)
     count = count + (Q - 1 - q) + one(jnp.logical_and(c == 1, q < Q - 1))
     pl.semaphore_wait(barrier, count)
 
@@ -780,12 +784,32 @@
     mine = block([])
     lines = share // 2
 
-    def fin_copy(h, core):
-        where = dev(q, c, g, y, core)
-        at = pl.ds(pl.multiple_of(core * lines, lines), lines)
-        return rdma(
-            fin.at[h, at, :], land.at[b, h], fin_send.at[h, core], fin_recv.at[b, h], where
-        )
+    def pass_copy(h):
+        at = pl.ds(pl.multiple_of((1 - c) * lines, lines), lines)
+        return rdma(fin.at[h, at, :], land.at[0, h], fin_send.at[h, 0], fin_recv.at[0, h], cdev)
+
+    def home_copies(h):
+        dim = plans[h][1][0]
+        found = []
+        for n, mask in enumerate(([], [dim])):
+            gg, tt = member(mask)
+            for core in range(2):
+                start = (gg * 2 + tt // 2) * share + core * lines
+                at = pl.ds(pl.multiple_of(start, lines), lines)
+                found.append(
+                    rdma(
+                        sbuf.at[h, at, :], land.at[1 + n, h], fin_send.at[h, 2 * n + core],
+                        fin_recv.at[1 + n, h], dev(q, c, gg, tt // 2, core),
+                    )
+                )
+        return found
+
+    def home_start(h):
+        dim = plans[h][1][0]
+        for mask in ([], [dim]):
+            sbuf[h, block(mask), :] = part[h, block(mask), :].astype(BF16)
+        for copy in home_copies(h):
+            copy.start()
 
     def columns(hb, h):
         start = chunk_at(h) * half
@@ -817,36 +841,37 @@
                     rs_start(h, 0)
     for h in range(CHUNKS):
         rs_finish(h, 0)
-        rs_start(h, 1)
-    for h in range(CHUNKS):
+        pl.when(first)(functools.partial(rs_start, h, 1))
+        pl.when(second)(functools.partial(home_start, h))
+    def last_sum(h):
         rs_finish(h, 1)
         fin[h] = part[h, mine, :].astype(BF16)
-
-        @pl.when(first)
-        def _():
-            fin_copy(h, 1 - c).start()
-            outb[:, columns(b, h)] = fin[h, pl.ds(pl.multiple_of(c * lines, lines), lines), :]
+        pass_copy(h).start()
+        outb[:, columns(b, h)] = fin[h, pl.ds(pl.multiple_of(c * lines, lines), lines), :]
+        put(b, h).start()
+
+    @pl.when(first)
+    def _():
+        for h in range(CHUNKS):
+            last_sum(h)
+
+
+    def arrived(i, h):
+        rdma(land.at[i, h], land.at[i, h], fin_send.at[h, 0], fin_recv.at[i, h], cdev).wait_recv()
+
+    for h in range(CHUNKS):
+        arrived(1, h)
+        arrived(2, h)
+        both = land[1, h].astype(F32) + land[2, h].astype(F32)
+        outb[:, columns(1 - b, h)] = both.astype(BF16)
+        put(1 - b, h).start()
+
+    @pl.when(second)
+    def _():
+        for h in range(CHUNKS):
+            arrived(0, h)
+            outb[:, columns(b, h)] = land[0, h]
             put(b, h).start()
-
-        @pl.when(second)
-        def _():
-            fin_copy(h, 0).start()
-            fin_copy(h, 1).start()
-
-
-    def take(hb, h):
-        rdma(
-            land.at[hb, h], land.at[hb, h], fin_send.at[h, 0], fin_recv.at[hb, h], cdev
-        ).wait_recv()
-        outb[:, columns(hb, h)] = land[hb, h]
-        put(hb, h).start()
-
-    for h in range(CHUNKS):
-        @pl.when(second)
-        def _():
-            take(b, h)
-
-        take(1 - b, h)
 
     for i in range(2):
         w_cross(i).wait_send()
@@ -900,18 +925,19 @@
             kv_pass(e, n).wait_send()
 
     for h in range(CHUNKS):
-        for dim, masks, base in plans[h]:
+        for i, (dim, masks, base) in enumerate(plans[h]):
             for n, mask in enumerate(masks):
-                rs_copy(h, dim, mask, base + n).wait_send()
+                copy = rs_copy(h, dim, mask, base + n)
+                pl.when(first)(copy.wait_send) if i else copy.wait_send()
 
         @pl.when(first)
         def _():
-            fin_copy(h, 1 - c).wait_send()
+            pass_copy(h).wait_send()
 
         @pl.when(second)
         def _():
-            fin_copy(h, 0).wait_send()
-            fin_copy(h, 1).wait_send()
+            for copy in home_copies(h):
+                copy.wait_send()
     for h in range(CHUNKS):
         for hb in range(2):
             put(hb, h).wait()
@@ -995,7 +1021,7 @@
             pltpu.VMEM((CHUNKS, rows, total_cols // 2 // CHUNKS), BF16),
             pltpu.VMEM((CHUNKS, members - 1, share, total_cols // 2 // CHUNKS), BF16),
             pltpu.VMEM((CHUNKS, share, total_cols // 2 // CHUNKS), BF16),
-            pltpu.VMEM((2, CHUNKS, share // 2, total_cols // 2 // CHUNKS), BF16),
+            pltpu.VMEM((3, CHUNKS, share // 2, total_cols // 2 // CHUNKS), BF16),
             pltpu.VMEM((rows // (G * tp), total_cols), BF16),
             dma((20,)),
             dma((2 * G * tp,)),
@@ -1017,8 +1043,8 @@
             dma((2,)),
             dma((CHUNKS, members - 1)),
             dma((CHUNKS, members - 1)),
-            dma((CHUNKS, 2)),
-            dma((2, CHUNKS)),
+            dma((CHUNKS, 4)),
+            dma((3, CHUNKS)),
             dma((2, CHUNKS)),
             dma((10,)),
         ],

time: 69.6 us -> 68.6 us (0.986)
  Pallas kernels: 67.8 us -> 66.7 us
    pallas_call x1, Pallas kernels: 67.8 us -> 66.7 us  [body(): pl.pallas_call(functools.partial(kernel, (G, Q, tp)), out_shape=jax.Shape...]
where the time goes in v5:
time: 68.6 us; the launch traced here: 68.4 us
  Pallas kernels  66.7 us (97%)
  local copies, waits for them, and re-layouts  1.67 us (2%)
    pallas_call x1, Pallas kernels, body(): pl.pallas_call(functools.partial(kernel, (G, Q, tp)), out_shape=jax.Shape...  66.7 us
    unnamed x1, local copies, waits for them, and re-layouts  1.67 us

profile of v5, /device:TPU:17, one launch (start us, length us, event | category | flops | bytes accessed | tf_op | source)
XLA Modules:
  0.0 68.4 jit_solution(11777947081040254658)
XLA Ops:
  0.0 66.7 %shard_map.145 = bf16[64,2048]{1,0:T(8,128)(2,1)} custom-call(bf16[256,512]{1,0:T(8,128)(2,1)} %tok_in.1, f32[4,1,512]{2,1,0:T(1,128)} %bitcast.3, bf16[256,128]{1,0:T(8,128)(2,1)} %q1_in.1, bf16[256,128]{1,0:T(8,128)(2,1)} %k1_in.1, bf16[256,128]{1,0:T(8,128)(2,1)} %q2_in.1, bf16[256,128]{1,0:T(8,128)(2,1)} %k2_in.1, bf16[256,256]{1,0:T(8,128)(2,1)} %v_in.1, ...), custom_call_target="tpu_custom_call" | custom-call | tf_op jit(solution)/shard_map/pallas_call | solution.py:985
  66.7 1.7 %copy.17 = bf16[64,2048]{1,0:T(8,128)(2,1)} copy(bf16[64,2048]{1,0:T(8,128)(2,1)} %shard_map.145) | data formatting | bytes 524288

commit v6 on v5

--- a/solution.py
+++ b/solution.py
@@ -19,7 +19,7 @@
 TAIL = 16
 CHUNKS = 8
 XY_HOME = (True, False)
-XY_PARTNER = (True, False)
+XY_PARTNER = (True, True)
 MESH = pl.DeviceIdType.MESH
 BF16 = jnp.bfloat16
 F32 = jnp.float32
@@ -279,7 +279,7 @@
     def w_pass(part_, slot, src=None):
         at = w_all.at[slot, :, shares[part_]]
         return rdma(
-            at if src is None else src, at, wd_send.at[part_ * S + slot],
+            at if src is None else src, at, wd_send,
             w_recv.at[part_ * slots + slot], cdev,
         )
 
@@ -371,11 +371,11 @@
     def o_pass(p, gg):
         at = o_at(c, p, gg)
         index = p * G + gg
-        return rdma(at, at, od_send.at[index], o_recv.at[c * S + index], cdev)
+        return rdma(at, at, od_send, o_recv.at[c * S + index], cdev)
 
     def o_wait(core, p, gg):
         at = o_at(core, p, gg)
-        rdma(at, at, od_send.at[0], o_recv.at[core * S + p * G + gg], cdev).wait_recv()
+        rdma(at, at, od_send, o_recv.at[core * S + p * G + gg], cdev).wait_recv()
 
     def o_own(kind):
         gg = g if kind == 0 else 1 - g
@@ -384,7 +384,7 @@
         def _():
             o_all[c, pl.ds(place_of(r, gg), cols), :] = op_ref[g] if kind == 0 else ox_ref[...]
             rdma(
-                op_ref.at[g] if kind == 0 else ox_ref, o_at(c, r, gg), od_send.at[r * G + gg],
+                op_ref.at[g] if kind == 0 else ox_ref, o_at(c, r, gg), od_send,
                 o_recv.at[c * S + r * G + gg], cdev,
             ).start()
 
@@ -420,7 +420,7 @@
 
     def w_wait(part_, slot):
         at = w_all.at[slot, :, shares[part_]]
-        rdma(at, at, wd_send.at[0], w_recv.at[part_ * slots + slot], cdev).wait_recv()
+        rdma(at, at, wd_send, w_recv.at[part_ * slots + slot], cdev).wait_recv()
 
     def early_relays(n):
         @pl.when(second)
@@ -759,7 +759,7 @@
     def rs_copy(h, dim, mask, index):
         at = block([dim] + mask)
         return rdma(
-            sbuf.at[h, at, :], rbuf.at[h, index], rs_send.at[h, index], rs_recv.at[h, index],
+            sbuf.at[h, at, :], rbuf.at[h, index], rs_send, rs_recv.at[h, index],
             device([dim]),
         )
 
@@ -786,7 +786,7 @@
 
     def pass_copy(h):
         at = pl.ds(pl.multiple_of((1 - c) * lines, lines), lines)
-        return rdma(fin.at[h, at, :], land.at[0, h], fin_send.at[h, 0], fin_recv.at[0, h], cdev)
+        return rdma(fin.at[h, at, :], land.at[0, h], fin_send, fin_recv.at[0, h], cdev)
 
     def home_copies(h):
         dim = plans[h][1][0]
@@ -798,7 +798,7 @@
                 at = pl.ds(pl.multiple_of(start, lines), lines)
                 found.append(
                     rdma(
-                        sbuf.at[h, at, :], land.at[1 + n, h], fin_send.at[h, 2 * n + core],
+                        sbuf.at[h, at, :], land.at[1 + n, h], fin_send,
                         fin_recv.at[1 + n, h], dev(q, c, gg, tt // 2, core),
                     )
                 )
@@ -817,7 +817,7 @@
 
     def put(hb, h):
         at = columns(hb, h)
-        return pltpu.make_async_copy(outb.at[:, at], out_ref.at[:, at], out_sem.at[hb, h])
+        return pltpu.make_async_copy(outb.at[:, at], out_ref.at[:, at], out_sem)
 
     for h in range(near):
         part[h] = part[h] + head_product(h, 1 - b)
@@ -857,7 +857,7 @@
 
 
     def arrived(i, h):
-        rdma(land.at[i, h], land.at[i, h], fin_send.at[h, 0], fin_recv.at[i, h], cdev).wait_recv()
+        rdma(land.at[i, h], land.at[i, h], fin_send, fin_recv.at[i, h], cdev).wait_recv()
 
     for h in range(CHUNKS):
         arrived(1, h)
@@ -877,13 +877,6 @@
         w_cross(i).wait_send()
         for kind in range(2):
             w_targets(lambda e: w_copy(i, kind, e).wait_send())
-
-    @pl.when(first)
-    def _():
-        @pl.loop(0, S)
-        def _(k):
-            w_pass(0, k).wait_send()
-            w_pass(1, k).wait_send()
 
     for n in range(2):
         for i in range(3):
@@ -908,13 +901,6 @@
     for kind in range(2):
         o_targets(lambda e: o_copy(kind, e).wait_send())
 
-    @pl.loop(0, R)
-    def _(p):
-        @pl.when(half_of(p) == b)
-        def _():
-            for gg in range(G):
-                o_pass(p, gg).wait_send()
-
     @pl.when(tail_out)
     def _():
         tail_copy.wait_send()
@@ -924,23 +910,22 @@
         def _(e):
             kv_pass(e, n).wait_send()
 
-    for h in range(CHUNKS):
-        for i, (dim, masks, base) in enumerate(plans[h]):
-            for n, mask in enumerate(masks):
-                copy = rs_copy(h, dim, mask, base + n)
-                pl.when(first)(copy.wait_send) if i else copy.wait_send()
-
-        @pl.when(first)
-        def _():
-            pass_copy(h).wait_send()
-
-        @pl.when(second)
-        def _():
-            for copy in home_copies(h):
-                copy.wait_send()
-    for h in range(CHUNKS):
-        for hb in range(2):
-            put(hb, h).wait()
+    def sent(src, sem):
+        rdma(src, src, sem, in_sem.at[0], cdev).wait_send()
+
+    @pl.when(first)
+    def _():
+        sent(w_all.at[0:S], wd_send)
+        sent(sbuf.at[0 : CHUNKS * 3 // 4], rs_send)
+        sent(fin.at[0 : CHUNKS // 2], fin_send)
+
+    @pl.when(second)
+    def _():
+        sent(sbuf.at[0 : CHUNKS // 2], rs_send)
+        sent(sbuf.at[0 : CHUNKS // 2], fin_send)
+
+    sent(o_all.at[0], od_send)
+    pltpu.make_async_copy(outb, out_ref, out_sem).wait()
 
 
 def body(
@@ -1027,10 +1012,10 @@
             dma((2 * G * tp,)),
             dma((4 * Q,)),
             dma((2,)),
-            dma((2 * sp,)),
+            dma,
             dma((2 * (sp + 1),)),
             dma((2 * Q,)),
-            dma((sp,)),
+            dma,
             dma((2 * sp,)),
             dma,
             dma,
@@ -1041,11 +1026,11 @@
             dma,
             dma((2,)),
             dma((2,)),
+            dma,
             dma((CHUNKS, members - 1)),
-            dma((CHUNKS, members - 1)),
-            dma((CHUNKS, 4)),
+            dma,
             dma((3, CHUNKS)),
-            dma((2, CHUNKS)),
+            dma,
             dma((10,)),
         ],
         compiler_params=pltpu.CompilerParams(

time: 68.6 us -> 67.4 us (0.983)
  Pallas kernels: 66.7 us -> 65.5 us
    pallas_call x1, Pallas kernels: 66.7 us -> 65.5 us  [body(): pl.pallas_call(functools.partial(kernel, (G, Q, tp)), out_shape=jax.Shape...]
where the time goes in v6:
time: 67.4 us; the launch traced here: 67.2 us
  Pallas kernels  65.5 us (97%)
  local copies, waits for them, and re-layouts  1.67 us (2%)
    pallas_call x1, Pallas kernels, body(): pl.pallas_call(functools.partial(kernel, (G, Q, tp)), out_shape=jax.Shape...  65.5 us
    unnamed x1, local copies, waits for them, and re-layouts  1.67 us

profile of v6, /device:TPU:17, one launch (start us, length us, event | category | flops | bytes accessed | tf_op | source)
XLA Modules:
  0.0 67.2 jit_solution(4577881079787310257)
XLA Ops:
  0.0 65.5 %shard_map.145 = bf16[64,2048]{1,0:T(8,128)(2,1)} custom-call(bf16[256,512]{1,0:T(8,128)(2,1)} %tok_in.1, f32[4,1,512]{2,1,0:T(1,128)} %bitcast.3, bf16[256,128]{1,0:T(8,128)(2,1)} %q1_in.1, bf16[256,128]{1,0:T(8,128)(2,1)} %k1_in.1, bf16[256,128]{1,0:T(8,128)(2,1)} %q2_in.1, bf16[256,128]{1,0:T(8,128)(2,1)} %k2_in.1, bf16[256,256]{1,0:T(8,128)(2,1)} %v_in.1, ...), custom_call_target="tpu_custom_call" | custom-call | tf_op jit(solution)/shard_map/pallas_call | solution.py:970
  65.5 1.7 %copy.17 = bf16[64,2048]{1,0:T(8,128)(2,1)} copy(bf16[64,2048]{1,0:T(8,128)(2,1)} %shard_map.145) | data formatting | bytes 524288
